TPU v7x, 32 devices: a whole 2x2x4 slice. The times are simulated.
32 devices in a mesh: row: 4 (over z), col: 8 (over y, x, core).
Axes of the slice: x: 2, y: 2, z: 4, core: 2. Of those that a mesh axis runs over, the one named last changes fastest.
Arguments:
- tokens: bfloat16 [32, 144, 2048], P('row', 'col'), may hold values from -6 to 6
- norm_gain: bfloat16 [2048], replicated, may hold values from 0.099609375 to 1.8984375
- w_in: bfloat16 [2048, 1152], replicated, may hold values from -0.125 to 0.125
- w_out: bfloat16 [1152, 2048], replicated, may hold values from -0.1875 to 0.1875
Outputs:
- mixed: bfloat16 [144, 32, 2048], P('row', 'col')
All inputs are finite; a program needn't handle non-finite values.
Results may differ from a plain program's by a relative error of at most 0.013.
Values may be sent and summed in bfloat16 or wider, within the bound.
No kernel may reach another device: no remote copies, remote signals or barrier semaphores. Data moves between devices by JAX's collectives and lax.ppermute only.
A program may use at most 64 MiB of HBM per device.

v0:
```python
import functools
import math

import jax
import jax.numpy as jnp
import numpy as np
from jax import lax
from jax.experimental import pallas as pl
from jax.experimental.pallas import tpu as pltpu
from jax.sharding import PartitionSpec as P

GROUP = 128


norm_eps = 1e-06
highest = lax.Precision.HIGHEST


def tables(length):
    series = jnp.arange(length, dtype=jnp.int32)
    product = series[:, None] * series[None, :] % length
    angles = product.astype(jnp.float32) * (2.0 * math.pi / length)
    return (jnp.cos(angles), jnp.sin(angles))


def folded_order(length_first, devices):
    block = length_first // devices
    half_block = block // 2
    series = jnp.arange(length_first, dtype=jnp.int32)
    device = series // block
    inner = series % block
    lower = device * half_block + inner
    upper = length_first - device * half_block - (inner - half_block)
    upper = jnp.where((device == 0) & (inner == half_block), length_first // 2, upper)
    return jnp.where(inner < half_block, lower, upper) % length_first


def to_channels(values, row_count):
    rows_first, rows_second, channels = values.shape
    width = channels // row_count
    parted = values.reshape(rows_first, rows_second, row_count, width).transpose(2, 0, 1, 3)
    return parted.reshape(row_count * rows_first, rows_second * width)


def product(table, values):
    return jnp.dot(table, values, precision=highest)


def middle(real_part, imag_part, width):
    length_first = real_part.shape[0]
    rows_second = real_part.shape[1] // width
    col_count = lax.axis_size("col")
    length_second = rows_second * col_count
    positions = length_first * length_second
    frequency = folded_order(length_first, col_count)
    series = jnp.arange(length_first, dtype=jnp.int32)
    first_angle = (frequency[:, None] * series[None, :] % length_first).astype(jnp.float32)
    first_angle = first_angle * (2.0 * math.pi / length_first)
    first_cos = jnp.cos(first_angle)
    first_sin = jnp.sin(first_angle)
    first_real = product(first_cos, real_part)
    first_imag = -product(first_sin, real_part)
    first_real = first_real + product(first_sin, imag_part)
    first_imag = first_imag + product(first_cos, imag_part)
    first_real = first_real.reshape(length_first, rows_second, width)
    first_imag = first_imag.reshape(length_first, rows_second, width)
    second_index = lax.axis_index("col") * rows_second + jnp.arange(rows_second, dtype=jnp.int32)
    twiddle_angle = (frequency[:, None] * second_index[None, :] % positions).astype(jnp.float32)
    twiddle_angle = twiddle_angle * (2.0 * math.pi / positions)
    twiddle_cos = jnp.cos(twiddle_angle)[:, :, None]
    twiddle_sin = jnp.sin(twiddle_angle)[:, :, None]
    turned_real = first_real * twiddle_cos + first_imag * twiddle_sin
    turned_imag = first_imag * twiddle_cos - first_real * twiddle_sin
    turned = jnp.stack([turned_real, turned_imag]).transpose(0, 2, 1, 3)
    turned = turned.reshape(2, rows_second, length_first * width)
    exchanged = lax.all_to_all(
        turned.astype(jnp.bfloat16), "col", split_axis=2, concat_axis=1, tiled=True
    ).astype(turned.dtype)
    second_cos, second_sin = tables(length_second)
    block = length_first // col_count
    out_shape = (length_second, block, width)
    out_real = (product(second_cos, exchanged[0]) + product(second_sin, exchanged[1])).reshape(
        out_shape
    )
    return out_real


def general(tokens, norm_gain, w_in, w_out):
    rows_first, rows_second, features = tokens.shape
    row_count = lax.axis_size("row")
    length_first = rows_first * row_count
    length_second = rows_second * lax.axis_size("col")
    channels = w_in.shape[1]
    width = channels // row_count
    groups = channels // GROUP
    scaling = 1.0 / math.sqrt(length_first * length_second * GROUP)
    floats = tokens.astype(jnp.float32)
    normed = (
        floats
        * lax.rsqrt(jnp.mean(floats * floats, axis=-1, keepdims=True) + norm_eps)
        * norm_gain.astype(jnp.float32)
    ).astype(jnp.bfloat16)
    mapped = jnp.dot(normed.reshape(-1, features), w_in, preferred_element_type=jnp.float32)
    mapped = mapped.astype(jnp.bfloat16).reshape(rows_first, rows_second, channels)
    channel_cos, channel_sin = tables(GROUP)
    grouped = mapped.astype(jnp.float32).reshape(rows_first, rows_second, groups, GROUP)
    spec_real = jnp.einsum("abgj,jm->abgm", grouped, channel_cos, precision=highest)
    spec_imag = -jnp.einsum("abgj,jm->abgm", grouped, channel_sin, precision=highest)
    stacked = jnp.stack(
        [
            to_channels(spec_real.reshape(rows_first, rows_second, channels), row_count),
            to_channels(spec_imag.reshape(rows_first, rows_second, channels), row_count),
        ]
    )
    arrived = lax.all_to_all(
        stacked.astype(jnp.bfloat16), "row", split_axis=1, concat_axis=1, tiled=True
    ).astype(stacked.dtype)
    result = middle(arrived[0], arrived[1], width)
    spectrum = (result * scaling).astype(jnp.bfloat16)
    returned = lax.all_to_all(spectrum, "row", split_axis=0, concat_axis=2, tiled=True)
    mixed = jnp.dot(returned.reshape(-1, channels), w_out, preferred_element_type=jnp.float32)
    return mixed.astype(jnp.bfloat16).reshape(returned.shape[0], returned.shape[1], features)


LANES = 128
TILE = 8
STEPS = 2
VMEM = pl.BlockSpec(memory_space=pltpu.VMEM)
HBM = pl.BlockSpec(memory_space=pltpu.HBM)


class Plan:
    def __init__(self, rows, cols, rows_first, rows_second, features, channels):
        self.rows, self.cols = rows, cols
        self.rows_first, self.rows_second = rows_first, rows_second
        self.features, self.channels = features, channels
        self.length_first = rows_first * rows
        self.length_second = rows_second * cols
        self.positions = self.length_first * self.length_second
        self.groups = channels // GROUP
        self.full = self.groups // rows
        self.sub = GROUP // rows
        self.half = rows_second // 2
        self.quads = -(-self.half // rows)
        self.tiles = self.full * self.half + self.quads
        self.local = rows_first * rows_second
        self.half_wide = rows // 2 * self.full * GROUP
        self.send_rows = self.full * self.local + 2 * self.quads * TILE
        self.pairs = self.length_first // cols // 2
        self.block_b = self.length_second // rows
        self.out_rows = self.block_b * 2 * self.pairs
        self.row_tiles = self.out_rows // TILE
        self.back_quads = -(-self.row_tiles // rows)
        self.back_rows = self.full * self.out_rows + self.back_quads * TILE

    def fits(self):
        return (
            GROUP == LANES
            and self.rows & (self.rows - 1) == 0
            and self.cols & (self.cols - 1) == 0
            and 1 < self.rows <= 8
            and self.cols > 1
            and self.rows_first == TILE
            and self.rows_second % 2 == 0
            and self.channels % GROUP == 0
            and self.groups % self.rows == 1
            and self.full == 2
            and self.length_first == 4 * self.cols
            and self.length_second % self.rows == 0
            and 2 * self.block_b % TILE == 0
            and self.features % 256 == 0
        )


def channel_table():
    j = np.arange(GROUP)[:, None]
    u = np.arange(GROUP)[None, :]
    half = GROUP // 2
    m = np.where(u <= half, u, u - half)
    angle = 2.0 * np.pi * (j * m % GROUP) / GROUP
    return np.where(u <= half, np.cos(angle), np.sin(angle))


def unfold_table():
    half = GROUP // 2
    table = np.zeros((GROUP, GROUP))
    for m in range(GROUP):
        near = m if m <= half else GROUP - m
        table[near, m] = 1.0
        if 0 < near < half:
            table[half + near, m] = -1.0 if m < half else 1.0
    return table


def paired(table):
    zero = np.zeros_like(table)
    return np.block([[table, zero], [zero, table]])


def first_tables(plan):
    a = np.arange(plan.length_first)
    out = np.zeros((plan.cols, plan.half, plan.cols, plan.pairs, 2, 2, 2, plan.length_first))
    for col in range(plan.cols):
        for b9 in range(plan.half):
            for h in range(2):
                b = col * plan.rows_second + h * plan.half + b9
                for c in range(plan.cols):
                    for i in range(plan.pairs):
                        k = c * plan.pairs + i
                        if k == 0:
                            out[col, b9, c, i, h, 0, h] = 1.0
                            out[col, b9, c, i, h, 1, h] = np.where(a % 2 == 0, 1.0, -1.0)
                        else:
                            phase = (a * plan.length_second + b) * k % plan.positions
                            angle = 2.0 * np.pi * phase / plan.positions
                            out[col, b9, c, i, h, 0, h] = np.cos(angle)
                            out[col, b9, c, i, h, 1, h] = -np.sin(angle)
    size = 2 * plan.length_first
    return out.reshape(plan.cols, plan.half, size, size)


def second_tables(plan):
    length = plan.length_second
    b9 = np.arange(plan.half)[:, None, None]
    c = np.arange(plan.cols)[None, :, None]
    h = np.arange(2)[None, None, :]
    b = (c * plan.rows_second + h * plan.half + b9).reshape(-1)
    k = np.arange(length)
    angle = 2.0 * np.pi * (k[:, None] * b[None, :] % length) / length
    cos, sin = np.cos(angle), np.sin(angle)
    cosine = np.stack([cos, sin], axis=-1)
    sine = np.stack([sin, -cos], axis=-1)

    def arrange(plus, minus):
        both = np.stack([plus, minus]).reshape(2, plan.rows, plan.block_b, -1)
        return both.transpose(1, 0, 2, 3).reshape(2 * length, -1)

    usual = np.stack([arrange(cosine, cosine[::-1]), arrange(sine, -sine[::-1])])
    turn = 2.0 * np.pi * ((plan.length_first // 2) * b % plan.positions) / plan.positions
    late = angle + turn[None, :]
    zero = np.zeros_like(cos)
    first = np.stack(
        [
            arrange(np.stack([cos, zero], -1), np.stack([zero, np.cos(late)], -1)),
            arrange(np.stack([sin, zero], -1), np.stack([zero, np.sin(late)], -1)),
        ]
    )
    return usual, first


def order_table(plan):
    table = np.zeros((plan.out_rows, plan.out_rows))
    for i in range(plan.pairs):
        for neg in range(2):
            for k in range(plan.block_b):
                row = (k * 2 + neg) * plan.pairs + i
                table[row, (i * 2 + neg) * plan.block_b + k] = 1.0
    return table


def dot(left, right):
    return jnp.dot(left, right, preferred_element_type=jnp.float32)


def lane_index(shape):
    return lax.broadcasted_iota(jnp.int32, shape, 1)


def turn_lanes(value, amount):
    amount = amount % LANES
    return value if amount == 0 else pltpu.roll(value, amount, 1)


def by_lane(pieces, sub):
    out = pieces[0]
    lane = lane_index(out.shape)
    for n in range(1, len(pieces)):
        out = jnp.where(lane >= n * sub, pieces[n], out)
    return out


def far_kernel(
    plan, depth, x_hbm, gain_hbm, w_hbm, table_hbm, out_ref, near_ref, normed_ref, x_ref, gain_ref, table_ref, w_ref, sems, w_sems
):
    wide = plan.half_wide
    other = 1 - lax.axis_index("row") // (plan.rows // 2)
    x_copy = pltpu.make_async_copy(x_hbm, x_ref, sems.at[0])
    gain_copy = pltpu.make_async_copy(gain_hbm, gain_ref, sems.at[1])
    table_copy = pltpu.make_async_copy(table_hbm, table_ref, sems.at[2])
    x_copy.start()
    gain_copy.start()
    steps = plan.features // depth
    copies = []
    for n in range(steps):
        rows = pl.ds(n * depth, depth)
        far = pltpu.make_async_copy(
            w_hbm.at[rows, pl.ds(pl.multiple_of(other * wide, LANES), wide)],
            w_ref.at[rows, pl.ds(0, wide)],
            w_sems.at[0, n],
        )
        last = pltpu.make_async_copy(
            w_hbm.at[rows, pl.ds(2 * wide, GROUP)], w_ref.at[rows, pl.ds(wide, GROUP)], w_sems.at[1, n]
        )
        far.start()
        last.start()
        copies.append((far, last))
    table_copy.start()
    gain_copy.wait()
    gain = gain_ref[...].astype(jnp.float32)
    x_copy.wait()
    step = 48 if plan.local % 48 == 0 else TILE
    for start in range(0, plan.local, step):
        rows = slice(start, start + step)
        total = jnp.zeros((step, LANES), jnp.float32)
        for n in range(plan.features // LANES):
            part = x_ref[rows, n * LANES : (n + 1) * LANES].astype(jnp.float32)
            total = total + part * part
        mean = jnp.sum(total, axis=-1, keepdims=True) * (1.0 / plan.features)
        scale = lax.rsqrt(mean + norm_eps)
        for n in range(plan.features // LANES):
            columns = slice(n * LANES, (n + 1) * LANES)
            part = x_ref[rows, columns].astype(jnp.float32)
            normed_ref[rows, columns] = (part * scale * gain[n : n + 1, :]).astype(jnp.bfloat16)
    total = None
    for n in range(steps):
        for copy in copies[n]:
            copy.wait()
        rows = slice(n * depth, (n + 1) * depth)
        part = dot(normed_ref[:, rows], w_ref[rows, :])
        total = part if n == 0 else total + part
    mapped = total.astype(jnp.bfloat16)
    table_copy.wait()
    values = dot(mapped[:, wide:], table_ref[:GROUP, :GROUP])
    sub, base = plan.sub, plan.full * plan.local
    turned = [turn_lanes(values, sub * t).astype(jnp.bfloat16) for t in range(plan.rows)]
    lower = other == 0
    for dest in range(plan.rows // 2):
        for h in range(2):
            for quad in range(plan.quads):
                ends = []
                for high in range(2):
                    pieces = []
                    for inner in range(plan.rows):
                        b9 = quad * plan.rows + inner
                        if b9 < plan.half:
                            row = (h * plan.half + b9) * TILE
                            turn = (inner - dest - high * (plan.rows // 2)) % plan.rows
                            pieces.append(turned[turn][row : row + TILE, :])
                    ends.append(by_lane(pieces, sub))
                at = (h * plan.quads + quad) * TILE
                out_ref[dest, base + at : base + at + TILE, :] = jnp.where(lower, ends[0], ends[1])
                near_ref[dest, at : at + TILE, :] = jnp.where(lower, ends[1], ends[0])
    spread(plan, mapped, table_ref, out_ref)


def spread(plan, mapped, table_ref, out_ref):
    for dest in range(plan.rows // 2):
        values = dot(mapped[:, dest * 2 * GROUP : (dest + 1) * 2 * GROUP], table_ref[...])
        for f in range(plan.full):
            out_ref[dest, f * plan.local : (f + 1) * plan.local, :] = values[
                :, f * GROUP : (f + 1) * GROUP
            ].astype(jnp.bfloat16)


def near_kernel(plan, depth, normed_ref, near_ref, w_hbm, table_hbm, out_ref, table_ref, w_ref, sem, w_sems):
    wide = plan.half_wide
    mine = lax.axis_index("row") // (plan.rows // 2)
    steps = plan.features // depth
    copies = []
    for n in range(steps):
        rows = pl.ds(n * depth, depth)
        copy = pltpu.make_async_copy(
            w_hbm.at[rows, pl.ds(pl.multiple_of(mine * wide, LANES), wide)], w_ref.at[rows, :], w_sems.at[n]
        )
        copy.start()
        copies.append(copy)
    table_copy = pltpu.make_async_copy(table_hbm, table_ref, sem)
    table_copy.start()
    out_ref[:, plan.full * plan.local :, :] = near_ref[...]
    total = None
    for n in range(steps):
        copies[n].wait()
        rows = slice(n * depth, (n + 1) * depth)
        part = dot(normed_ref[:, rows], w_ref[rows, :])
        total = part if n == 0 else total + part
    table_copy.wait()
    spread(plan, total.astype(jnp.bfloat16), table_ref, out_ref)


def first_kernel(plan, *refs):
    slabs, (table_ref, out_ref, held_ref) = refs[: plan.rows], refs[plan.rows :]
    row = lax.axis_index("row")
    for s in range(plan.rows):
        held_ref[row ^ s] = slabs[s][...]
    for b9 in range(plan.half):
        quad, inner = divmod(b9, plan.rows)
        columns = []
        for f in range(plan.full):
            parts = []
            for h in range(2):
                at = f * plan.local + (h * plan.half + b9) * TILE
                parts += [held_ref[r, at : at + TILE, :] for r in range(plan.rows)]
            columns.append(jnp.concatenate(parts, axis=0))
        parts = []
        for h in range(2):
            at = plan.full * plan.local + (h * plan.quads + quad) * TILE
            parts += [held_ref[r, at : at + TILE, :] for r in range(plan.rows)]
        columns.append(jnp.concatenate(parts, axis=0))
        result = dot(table_ref[b9], jnp.concatenate(columns, axis=1))
        for f in range(plan.full):
            at = (f * plan.half + b9) * TILE
            piece = result[:, f * LANES : (f + 1) * LANES].astype(jnp.bfloat16)
            for c in range(plan.cols):
                out_ref[c, at : at + TILE, :] = piece[c * TILE : (c + 1) * TILE, :]
        tail = result[:, plan.full * LANES :]
        packed = tail if inner == 0 else jnp.where(lane_index(tail.shape) >= inner * plan.sub, tail, packed)
        if inner == plan.rows - 1 or b9 == plan.half - 1:
            at = (plan.full * plan.half + quad) * TILE
            piece = packed.astype(jnp.bfloat16)
            for c in range(plan.cols):
                out_ref[c, at : at + TILE, :] = piece[c * TILE : (c + 1) * TILE, :]


def second_kernel(plan, scaling, *refs):
    slabs = refs[: plan.cols]
    usual_ref, first_ref, out_ref, held_ref, rhs_ref = refs[plan.cols :]
    row, col = lax.axis_index("row"), lax.axis_index("col")
    for s in range(plan.cols):
        held_ref[col ^ s] = slabs[s][...]
    sub, quarter = plan.sub, TILE // 2
    low = lax.broadcasted_iota(jnp.int32, (TILE, LANES), 0) < quarter
    for b9 in range(plan.half):
        quad, inner = divmod(b9, plan.rows)
        places = [(f * plan.half + b9) * TILE for f in range(plan.full)]
        places.append((plan.full * plan.half + quad) * TILE)
        for p in range(plan.cols // 2):
            at = b9 * (plan.cols // 2) * TILE + p * TILE
            for n, place in enumerate(places):
                even = held_ref[2 * p, place : place + TILE, :].astype(jnp.float32)
                odd = held_ref[2 * p + 1, place : place + TILE, :].astype(jnp.float32)
                both = [
                    jnp.where(low, even, pltpu.roll(odd, quarter, 0)),
                    jnp.where(low, pltpu.roll(even, quarter, 0), odd),
                ]
                for i in range(plan.pairs):
                    value = both[i]
                    if n == plan.full:
                        value = turn_lanes(value, -inner * sub)
                    rhs_ref[i, at : at + TILE, n * LANES : (n + 1) * LANES] = value.astype(jnp.bfloat16)
    wide = (plan.full + 1) * LANES
    lane = lane_index((1, wide))
    last = lane >= plan.full * LANES
    place = jnp.where(last, lane - plan.full * LANES + row * sub, lane & (LANES - 1))
    is_sine = place > GROUP // 2
    span = 2 * plan.block_b
    kept = {}
    for i in range(plan.pairs):
        table = first_ref if i == 0 else usual_ref
        values = rhs_ref[i]
        for r in range(plan.rows):
            cosine = dot(table[0, r * span : (r + 1) * span, :], values)
            sine = dot(table[1, r * span : (r + 1) * span, :], values)
            merged = jnp.where(is_sine, sine, cosine) * scaling
            for f in range(plan.full):
                at = f * plan.out_rows + i * span
                out_ref[r, at : at + span, :] = merged[:, f * LANES : (f + 1) * LANES].astype(jnp.bfloat16)
            tail = merged[:, plan.full * LANES :]
            for t in range(span // TILE):
                whole, inner = divmod(i * (span // TILE) + t, plan.rows)
                at = plan.full * plan.out_rows + whole * TILE
                piece = turn_lanes(tail[t * TILE : (t + 1) * TILE, :], inner * sub)
                if inner:
                    piece = jnp.where(lane_index(piece.shape) >= inner * sub, piece, kept[r])
                kept[r] = piece
                if inner == plan.rows - 1 or (i == plan.pairs - 1 and t == span // TILE - 1):
                    out_ref[r, at : at + TILE, :] = piece.astype(jnp.bfloat16)


def tail_kernel(plan, *refs):
    slabs = refs[: plan.rows]
    unfold_ref, order_ref, w_ref, out_ref, held_ref, spectrum_ref = refs[plan.rows :]
    row = lax.axis_index("row")
    for s in range(plan.rows):
        held_ref[row ^ s] = slabs[s][...]
    order = order_ref[...]
    unfold = unfold_ref[...]
    for q in range(plan.rows):
        pair = [held_ref[q, f * plan.out_rows : (f + 1) * plan.out_rows, :] for f in range(plan.full)]
        ordered = dot(order, jnp.concatenate(pair, axis=1)).astype(jnp.bfloat16)
        spectrum_ref[:, q * 2 * GROUP : (q + 1) * 2 * GROUP] = dot(ordered, unfold).astype(jnp.bfloat16)
    base = plan.full * plan.out_rows
    packed = [held_ref[q, base:, :].astype(jnp.float32) for q in range(plan.rows)]
    turned = [[turn_lanes(value, plan.sub * t) for t in range(plan.rows)] for value in packed]
    pieces = []
    for t in range(plan.row_tiles):
        whole, inner = divmod(t, plan.rows)
        rows = slice(whole * TILE, (whole + 1) * TILE)
        pieces.append(
            by_lane([turned[q][(q - inner) % plan.rows][rows, :] for q in range(plan.rows)], plan.sub)
        )
    last = jnp.concatenate(pieces, axis=0).astype(jnp.bfloat16)
    ordered = dot(order, last).astype(jnp.bfloat16)
    spectrum_ref[:, plan.rows * 2 * GROUP :] = dot(ordered, unfold[:GROUP, :GROUP]).astype(jnp.bfloat16)
    wide = 256
    group = 2 * plan.pairs
    for n in range(plan.features // wide):
        columns = slice(n * wide, (n + 1) * wide)
        result = dot(spectrum_ref[...], w_ref[:, columns]).astype(jnp.bfloat16)
        for k in range(plan.block_b):
            out_ref[k, :, columns] = result[k * group : (k + 1) * group, :]


def estimate(flops, moved):
    return pl.CostEstimate(flops=flops, bytes_accessed=moved, transcendentals=0)


def limit(mebibytes):
    return pltpu.CompilerParams(vmem_limit_bytes=mebibytes * 2**20)


def exchange(values, axis, size):
    here = lax.axis_index(axis)
    out = []
    for s in range(size):
        if isinstance(values, tuple):
            source, index = values[2 * s // size], (here ^ s) % (size // 2)
        else:
            source, index = values, here ^ s
        slab = lax.dynamic_index_in_dim(source, index, 0, keepdims=False)
        if s:
            slab = lax.ppermute(slab, axis, [(n, n ^ s) for n in range(size)])
        out.append(slab)
    return out


def fetch_kernel(w_hbm, after_ref, w_ref, sem):
    copy = pltpu.make_async_copy(w_hbm, w_ref, sem)
    copy.start()
    copy.wait()


def fetch(w_out, after):
    return pl.pallas_call(
        fetch_kernel,
        out_shape=pltpu.VMEM(w_out.shape, w_out.dtype),
        in_specs=[HBM, VMEM],
        out_specs=VMEM,
        scratch_shapes=[pltpu.SemaphoreType.DMA],
        compiler_params=limit(2),
        cost_estimate=estimate(10**9, 2 * w_out.size),
        name="fetch",
    )(pltpu.with_memory_space_constraint(w_out, pltpu.HBM), after)


def packed(plan, tokens, norm_gain, w_in, w_out):
    half_type = jnp.bfloat16
    scaling = 1.0 / math.sqrt(plan.positions * GROUP)
    col = lax.axis_index("col")
    local, features, channels = plan.local, plan.features, plan.channels
    x = tokens.transpose(1, 0, 2).reshape(local, features)
    channel = jnp.asarray(paired(channel_table()), half_type)
    gain = norm_gain.reshape(features // LANES, LANES)
    x, gain, w_in, channel = (pltpu.with_memory_space_constraint(v, pltpu.HBM) for v in (x, gain, w_in, channel))
    depth, wide = features // STEPS, plan.half_wide
    packed_rows = 2 * plan.quads * TILE
    far, near, normed = pl.pallas_call(
        functools.partial(far_kernel, plan, depth),
        out_shape=(
            pltpu.VMEM((plan.rows // 2, plan.send_rows, LANES), half_type),
            pltpu.VMEM((plan.rows // 2, packed_rows, LANES), half_type),
            pltpu.VMEM((local, features), half_type),
        ),
        in_specs=[HBM] * 4,
        out_specs=(VMEM, VMEM, VMEM),
        scratch_shapes=[
            pltpu.VMEM((local, features), half_type),
            pltpu.VMEM((features // LANES, LANES), half_type),
            pltpu.VMEM((2 * GROUP, 2 * GROUP), half_type),
            pltpu.VMEM((features, wide + GROUP), half_type),
            pltpu.SemaphoreType.DMA((3,)),
            pltpu.SemaphoreType.DMA((2, STEPS)),
        ],
        compiler_params=pltpu.CompilerParams(vmem_limit_bytes=16 * 2**20),
        cost_estimate=estimate(local * features * channels, features * channels),
        name="far",
    )(x, gain, w_in, channel)
    close = pl.pallas_call(
        functools.partial(near_kernel, plan, depth),
        out_shape=pltpu.VMEM((plan.rows // 2, plan.send_rows, LANES), half_type),
        in_specs=[VMEM, VMEM, HBM, HBM],
        out_specs=VMEM,
        scratch_shapes=[
            pltpu.VMEM((2 * GROUP, 2 * GROUP), half_type),
            pltpu.VMEM((features, wide), half_type),
            pltpu.SemaphoreType.DMA,
            pltpu.SemaphoreType.DMA((STEPS,)),
        ],
        compiler_params=pltpu.CompilerParams(vmem_limit_bytes=8 * 2**20),
        cost_estimate=estimate(local * features * channels, features * channels),
        name="near",
    )(normed, near, w_in, channel)
    slabs = exchange((close, far), "row", plan.rows)
    first = lax.dynamic_index_in_dim(jnp.asarray(first_tables(plan), half_type), col, 0, keepdims=False)
    turned = pl.pallas_call(
        functools.partial(first_kernel, plan),
        out_shape=jax.ShapeDtypeStruct((plan.cols, plan.tiles * TILE, LANES), half_type),
        in_specs=[VMEM] * (plan.rows + 1),
        out_specs=VMEM,
        scratch_shapes=[pltpu.VMEM((plan.rows, plan.send_rows, LANES), half_type)],
        compiler_params=limit(8),
        cost_estimate=estimate(10**8, 10**6),
        name="first",
    )(*slabs, first)
    slabs = exchange(turned, "col", plan.cols)
    usual, special = (jnp.asarray(table, half_type) for table in second_tables(plan))
    leading = jnp.where(col == 0, special, usual)
    depth = plan.half * plan.cols * 4
    back = pl.pallas_call(
        functools.partial(second_kernel, plan, scaling),
        out_shape=jax.ShapeDtypeStruct((plan.rows, plan.back_rows, LANES), half_type),
        in_specs=[VMEM] * (plan.cols + 2),
        out_specs=VMEM,
        scratch_shapes=[
            pltpu.VMEM((plan.cols, plan.tiles * TILE, LANES), half_type),
            pltpu.VMEM((plan.pairs, depth, (plan.full + 1) * LANES), half_type),
        ],
        compiler_params=limit(12),
        cost_estimate=estimate(3 * 10**8, 10**6),
        name="second",
    )(*slabs, usual, leading)
    slabs = exchange(back, "row", plan.rows)
    w_out = fetch(w_out, slabs[0][:TILE])
    return pl.pallas_call(
        functools.partial(tail_kernel, plan),
        out_shape=jax.ShapeDtypeStruct((plan.block_b, 2 * plan.pairs, features), half_type),
        in_specs=[VMEM] * (plan.rows + 3),
        out_specs=VMEM,
        scratch_shapes=[
            pltpu.VMEM((plan.rows, plan.back_rows, LANES), half_type),
            pltpu.VMEM((plan.out_rows, channels), half_type),
        ],
        compiler_params=limit(12),
        cost_estimate=estimate(2 * local * features * channels, 2 * features * channels),
        name="tail",
    )(*slabs, jnp.asarray(paired(unfold_table()), half_type), jnp.asarray(order_table(plan), half_type), w_out)


def shards(tokens, norm_gain, w_in, w_out):
    rows_first, rows_second, features = tokens.shape
    plan = Plan(
        lax.axis_size("row"), lax.axis_size("col"), rows_first, rows_second, features, w_in.shape[1]
    )
    if plan.fits():
        return packed(plan, tokens, norm_gain, w_in, w_out)
    return general(tokens, norm_gain, w_in, w_out)


def solution(mesh):
    in_specs = (P("row", "col", None), P(), P(), P())
    out_specs = P("row", "col", None)

    return jax.shard_map(shards, mesh=mesh, in_specs=in_specs, out_specs=out_specs, check_vma=False)
```

profile of v0, /device:TPU:0, one launch (start us, length us, event | category | flops | bytes accessed | tf_op | source)
XLA Modules:
  0.0 42.1 jit_solution(10265738550908228243)
XLA Ops:
  0.0 2.9 %far.1 = (bf16[2,336,128]{2,1,0:T(8,128)(2,1)S(1)}, bf16[2,48,128]{2,1,0:T(8,128)(2,1)S(1)}, bf16[144,2048]{1,0:T(8,128)(2,1)S(1)}) custom-call(bf16[144,2048]{1,0:T(8,128)(2,1)} %bitcast.40, bf16[16,128]{1,0:T(8,128)(2,1)} %bitcast.41, bf16[2048,1152]{1,0:T(8,128)(2,1)} %w_hbm.4, bf16[256,256]{1,0:T(8,128)(2,1)} %constant.100.clone.table_hbm), custom_call_target="tpu_custom_call" | custom-call | flops 339738624 | bytes 2359296 | tf_op jit(solution)/shard_map/far/pallas_call | solution.py:566
  2.9 0.0 copy-start
  2.9 0.0 copy-start.3
  2.9 2.4 %near.1 = bf16[2,336,128]{2,1,0:T(8,128)(2,1)S(1)} custom-call(bf16[144,2048]{1,0:T(8,128)(2,1)S(1)} %get-tuple-element.8.normed_ref, bf16[2,48,128]{2,1,0:T(8,128)(2,1)S(1)} %get-tuple-element.9.near_ref, bf16[2048,1152]{1,0:T(8,128)(2,1)} %w_hbm.4, bf16[256,256]{1,0:T(8,128)(2,1)} %constant.100.clone.table_hbm), custom_call_target="tpu_custom_call" | custom-call | flops 339738624 | bytes 2359296 | tf_op jit(solution)/shard_map/near/pallas_call | solution.py:587
  5.4 3.1 %collective-permute-start = (bf16[336,128]{1,0:T(8,128)(2,1)S(1)}, bf16[336,128]{1,0:T(8,128)(2,1)S(1)}, u32[]{:S(2)}, u32[]{:S(2)}) collective-permute-start(bf16[336,128]{1,0:T(8,128)(2,1)S(1)} %get-tuple-element.25), channel_id=1, source_target_pairs={{0,8},{8,0},{16,24},{24,16},{1,9},{9,1},{17,25},{25,17},{2,10},{10... | collective-permute-start | bytes 258056 | tf_op jit(solution)/shard_map/ppermute | solution.py:531
  8.5 2.6 %collective-permute-start.2 = (bf16[336,128]{1,0:T(8,128)(2,1)S(1)}, bf16[336,128]{1,0:T(8,128)(2,1)S(1)}, u32[]{:S(2)}, u32[]{:S(2)}) collective-permute-start(bf16[336,128]{1,0:T(8,128)(2,1)S(1)} %get-tuple-element.23), channel_id=1, source_target_pairs={{0,24},{8,16},{16,8},{24,0},{1,25},{9,17},{17,9},{25,1},{2,26},{10... | collective-permute-start | bytes 258056 | tf_op jit(solution)/shard_map/ppermute | solution.py:531
  11.0 0.2 collective-permute-start.1
  11.2 0.9 %dynamic-slice_bitcast_fusion.refs_4_ = bf16[9,64,64]{2,1,0:T(8,128)(2,1)S(1)} fusion(bf16[8,9,64,64]{3,2,1,0:T(8,128)(2,1)} %constant.101.clone, s32[]{:T(128)S(6)} %select_n.88), kind=kLoop, calls=%fused_computation.1 | loop fusion | bytes 147460 | tf_op jit(solution)/shard_map/jit(dynamic_index_in_dim)/squeeze | solution.py:603
  12.2 4.1 %collective-permute-done.2.refs_3_ = bf16[336,128]{1,0:T(8,128)(2,1)S(1)} collective-permute-done((bf16[336,128]{1,0:T(8,128)(2,1)S(1)}, bf16[336,128]{1,0:T(8,128)(2,1)S(1)}, u32[]{:S(2)}, u32[]{:S(2)}) %collective-permute-start.2) | collective-permute-done | bytes 86048 | tf_op jit(solution)/shard_map/ppermute | solution.py:531
  16.3 2.8 %collective-permute-done.1.refs_2_ = bf16[336,128]{1,0:T(8,128)(2,1)S(1)} collective-permute-done((bf16[336,128]{1,0:T(8,128)(2,1)S(1)}, bf16[336,128]{1,0:T(8,128)(2,1)S(1)}, u32[]{:S(2)}, u32[]{:S(2)}) %collective-permute-start.1) | collective-permute-done | bytes 86048 | tf_op jit(solution)/shard_map/ppermute | solution.py:531
  19.1 0.3 first.1
  19.4 1.9 %collective-permute-start.9 = (bf16[168,128]{1,0:T(8,128)(2,1)S(1)}, bf16[168,128]{1,0:T(8,128)(2,1)S(1)}, u32[]{:S(2)}, u32[]{:S(2)}) collective-permute-start(bf16[168,128]{1,0:T(8,128)(2,1)S(1)} %get-tuple-element.11), channel_id=1, source_target_pairs={{0,7},{1,6},{2,5},{3,4},{4,3},{5,2},{6,1},{7,0},{8,15},{9,14},{10,... | collective-permute-start | bytes 129032 | tf_op jit(solution)/shard_map/ppermute | solution.py:531
  21.3 0.7 %collective-permute-start.8 = (bf16[168,128]{1,0:T(8,128)(2,1)S(1)}, bf16[168,128]{1,0:T(8,128)(2,1)S(1)}, u32[]{:S(2)}, u32[]{:S(2)}) collective-permute-start(bf16[168,128]{1,0:T(8,128)(2,1)S(1)} %get-tuple-element.12), channel_id=1, source_target_pairs={{0,6},{1,7},{2,4},{3,5},{4,2},{5,3},{6,0},{7,1},{8,14},{9,15},{10,... | collective-permute-start | bytes 129032 | tf_op jit(solution)/shard_map/ppermute | solution.py:531
  22.0 1.4 %collective-permute-start.7 = (bf16[168,128]{1,0:T(8,128)(2,1)S(1)}, bf16[168,128]{1,0:T(8,128)(2,1)S(1)}, u32[]{:S(2)}, u32[]{:S(2)}) collective-permute-start(bf16[168,128]{1,0:T(8,128)(2,1)S(1)} %get-tuple-element.13), channel_id=1, source_target_pairs={{0,5},{1,4},{2,7},{3,6},{4,1},{5,0},{6,3},{7,2},{8,13},{9,12},{10,... | collective-permute-start | bytes 129032 | tf_op jit(solution)/shard_map/ppermute | solution.py:531
  23.4 0.5 %collective-permute-start.6 = (bf16[168,128]{1,0:T(8,128)(2,1)S(1)}, bf16[168,128]{1,0:T(8,128)(2,1)S(1)}, u32[]{:S(2)}, u32[]{:S(2)}) collective-permute-start(bf16[168,128]{1,0:T(8,128)(2,1)S(1)} %get-tuple-element.14), channel_id=1, source_target_pairs={{0,4},{1,5},{2,6},{3,7},{4,0},{5,1},{6,2},{7,3},{8,12},{9,13},{10,... | collective-permute-start | bytes 129032 | tf_op jit(solution)/shard_map/ppermute | solution.py:531
  23.9 0.8 %collective-permute-start.5 = (bf16[168,128]{1,0:T(8,128)(2,1)S(1)}, bf16[168,128]{1,0:T(8,128)(2,1)S(1)}, u32[]{:S(2)}, u32[]{:S(2)}) collective-permute-start(bf16[168,128]{1,0:T(8,128)(2,1)S(1)} %get-tuple-element.15), channel_id=1, source_target_pairs={{0,3},{1,2},{2,1},{3,0},{4,7},{5,6},{6,5},{7,4},{8,11},{9,10},{10,... | collective-permute-start | bytes 129032 | tf_op jit(solution)/shard_map/ppermute | solution.py:531
  24.7 1.0 %collective-permute-start.4 = (bf16[168,128]{1,0:T(8,128)(2,1)S(1)}, bf16[168,128]{1,0:T(8,128)(2,1)S(1)}, u32[]{:S(2)}, u32[]{:S(2)}) collective-permute-start(bf16[168,128]{1,0:T(8,128)(2,1)S(1)} %get-tuple-element.16), channel_id=1, source_target_pairs={{0,2},{1,3},{2,0},{3,1},{4,6},{5,7},{6,4},{7,5},{8,10},{9,11},{10,... | collective-permute-start | bytes 129032 | tf_op jit(solution)/shard_map/ppermute | solution.py:531
  25.7 0.9 %collective-permute-done.8.refs_6_ = bf16[168,128]{1,0:T(8,128)(2,1)S(1)} collective-permute-done((bf16[168,128]{1,0:T(8,128)(2,1)S(1)}, bf16[168,128]{1,0:T(8,128)(2,1)S(1)}, u32[]{:S(2)}, u32[]{:S(2)}) %collective-permute-start.8) | collective-permute-done | bytes 43040 | tf_op jit(solution)/shard_map/ppermute | solution.py:531
  26.6 0.1 broadcast_select_fusion.refs_9_
  26.7 0.0 collective-permute-done.7.refs_5_
  26.7 1.1 %collective-permute-done.6.refs_4_ = bf16[168,128]{1,0:T(8,128)(2,1)S(1)} collective-permute-done((bf16[168,128]{1,0:T(8,128)(2,1)S(1)}, bf16[168,128]{1,0:T(8,128)(2,1)S(1)}, u32[]{:S(2)}, u32[]{:S(2)}) %collective-permute-start.6) | collective-permute-done | bytes 43040 | tf_op jit(solution)/shard_map/ppermute | solution.py:531
  27.8 1.2 %collective-permute-done.4.refs_2_ = bf16[168,128]{1,0:T(8,128)(2,1)S(1)} collective-permute-done((bf16[168,128]{1,0:T(8,128)(2,1)S(1)}, bf16[168,128]{1,0:T(8,128)(2,1)S(1)}, u32[]{:S(2)}, u32[]{:S(2)}) %collective-permute-start.4) | collective-permute-done | bytes 43040 | tf_op jit(solution)/shard_map/ppermute | solution.py:531
  29.0 0.0 collective-permute-done.3.refs_1_
  29.0 1.2 %second.1 = bf16[4,328,128]{2,1,0:T(8,128)(2,1)S(1)} custom-call(bf16[168,128]{1,0:T(8,128)(2,1)S(1)} %get-tuple-element.18.refs_0_, bf16[168,128]{1,0:T(8,128)(2,1)S(1)} %collective-permute-done.3.refs_1_, bf16[168,128]{1,0:T(8,128)(2,1)S(1)} %collective-permute-done.4.refs_2_, bf16[168,128]{1,0:T(8,128)(2,1)S(1)} %collective-permute-done.5.refs_3_, ...), custom_call_target="tpu_custom_call" | custom-call | flops 300000000 | bytes 1000000 | tf_op jit(solution)/shard_map/second/pallas_call | solution.py:618
  30.3 2.6 %collective-permute-start.12 = (bf16[328,128]{1,0:T(8,128)(2,1)S(1)}, bf16[328,128]{1,0:T(8,128)(2,1)S(1)}, u32[]{:S(2)}, u32[]{:S(2)}) collective-permute-start(bf16[328,128]{1,0:T(8,128)(2,1)S(1)} %get-tuple-element.19), channel_id=1, source_target_pairs={{0,24},{8,16},{16,8},{24,0},{1,25},{9,17},{17,9},{25,1},{2,26},{10... | collective-permute-start | bytes 251912 | tf_op jit(solution)/shard_map/ppermute | solution.py:531
  32.9 0.0 collective-permute-start.11
  32.9 1.9 %collective-permute-start.10 = (bf16[328,128]{1,0:T(8,128)(2,1)S(1)}, bf16[328,128]{1,0:T(8,128)(2,1)S(1)}, u32[]{:S(2)}, u32[]{:S(2)}) collective-permute-start(bf16[328,128]{1,0:T(8,128)(2,1)S(1)} %get-tuple-element.21), channel_id=1, source_target_pairs={{0,8},{8,0},{16,24},{24,16},{1,9},{9,1},{17,25},{25,17},{2,10},{10... | collective-permute-start | bytes 251912 | tf_op jit(solution)/shard_map/ppermute | solution.py:531
  34.8 2.3 %fetch.1.refs_6_ = bf16[1152,2048]{1,0:T(8,128)(2,1)S(1)} custom-call(bf16[1152,2048]{1,0:T(8,128)(2,1)} %w_hbm.5, bf16[8,128]{1,0:T(8,128)(2,1)S(1)} %fusion.after_ref), custom_call_target="tpu_custom_call" | custom-call | flops 1000000000 | bytes 4718592 | tf_op jit(solution)/shard_map/fetch/pallas_call | solution.py:543
  37.1 0.4 collective-permute-done.12.refs_3_
  37.5 2.6 %collective-permute-done.11.refs_2_ = bf16[328,128]{1,0:T(8,128)(2,1)S(1)} collective-permute-done((bf16[328,128]{1,0:T(8,128)(2,1)S(1)}, bf16[328,128]{1,0:T(8,128)(2,1)S(1)}, u32[]{:S(2)}, u32[]{:S(2)}) %collective-permute-start.11) | collective-permute-done | bytes 84000 | tf_op jit(solution)/shard_map/ppermute | solution.py:531
  40.1 0.0 collective-permute-done.10.refs_1_
  40.1 2.1 %tail.1 = bf16[36,4,2048]{2,1,0:T(4,128)(2,1)} custom-call(bf16[328,128]{1,0:T(8,128)(2,1)S(1)} %get-tuple-element.22.refs_0_, bf16[328,128]{1,0:T(8,128)(2,1)S(1)} %collective-permute-done.10.refs_1_, bf16[328,128]{1,0:T(8,128)(2,1)S(1)} %collective-permute-done.11.refs_2_, bf16[328,128]{1,0:T(8,128)(2,1)S(1)} %collective-permute-done.12.refs_3_, ...), custom_call_target="tpu_custom_call" | custom-call | flops 679477248 | bytes 4718592 | tf_op jit(solution)/shard_map/tail/pallas_call | solution.py:633
  (15 shorter events, 0.1 us)
Async XLA Ops:
  2.9 23.7 %copy-start = (bf16[2,288,288]{2,1,0:T(8,128)(2,1)S(1)}, bf16[2,288,288]{2,1,0:T(8,128)(2,1)}, u32[]{:S(2)}) copy-start(bf16[2,288,288]{2,1,0:T(8,128)(2,1)} %constant.102.clone.refs_8_) | copy-start | bytes 995332
  2.9 23.7 %copy-start.3 = (bf16[2,288,288]{2,1,0:T(8,128)(2,1)S(1)}, bf16[2,288,288]{2,1,0:T(8,128)(2,1)}, u32[]{:S(2)}) copy-start(bf16[2,288,288]{2,1,0:T(8,128)(2,1)} %constant.103.clone) | copy-start | bytes 995332
  5.4 6.8 %collective-permute-start = (bf16[336,128]{1,0:T(8,128)(2,1)S(1)}, bf16[336,128]{1,0:T(8,128)(2,1)S(1)}, u32[]{:S(2)}, u32[]{:S(2)}) collective-permute-start(bf16[336,128]{1,0:T(8,128)(2,1)S(1)} %get-tuple-element.25), channel_id=1, source_target_pairs={{0,8},{8,0},{16,24},{24,16},{1,9},{9,1},{17,25},{25,17},{2,10},{10... | collective-permute-start | bytes 258056 | tf_op jit(solution)/shard_map/ppermute | solution.py:531
  8.5 7.8 %collective-permute-start.2 = (bf16[336,128]{1,0:T(8,128)(2,1)S(1)}, bf16[336,128]{1,0:T(8,128)(2,1)S(1)}, u32[]{:S(2)}, u32[]{:S(2)}) collective-permute-start(bf16[336,128]{1,0:T(8,128)(2,1)S(1)} %get-tuple-element.23), channel_id=1, source_target_pairs={{0,24},{8,16},{16,8},{24,0},{1,25},{9,17},{17,9},{25,1},{2,26},{10... | collective-permute-start | bytes 258056 | tf_op jit(solution)/shard_map/ppermute | solution.py:531
  11.0 8.0 %collective-permute-start.1 = (bf16[336,128]{1,0:T(8,128)(2,1)S(1)}, bf16[336,128]{1,0:T(8,128)(2,1)S(1)}, u32[]{:S(2)}, u32[]{:S(2)}) collective-permute-start(bf16[336,128]{1,0:T(8,128)(2,1)S(1)} %get-tuple-element.24), channel_id=1, source_target_pairs={{0,16},{8,24},{16,0},{24,8},{1,17},{9,25},{17,1},{25,9},{2,18},{10... | collective-permute-start | bytes 258056 | tf_op jit(solution)/shard_map/ppermute | solution.py:531
  19.4 5.3 %collective-permute-start.9 = (bf16[168,128]{1,0:T(8,128)(2,1)S(1)}, bf16[168,128]{1,0:T(8,128)(2,1)S(1)}, u32[]{:S(2)}, u32[]{:S(2)}) collective-permute-start(bf16[168,128]{1,0:T(8,128)(2,1)S(1)} %get-tuple-element.11), channel_id=1, source_target_pairs={{0,7},{1,6},{2,5},{3,4},{4,3},{5,2},{6,1},{7,0},{8,15},{9,14},{10,... | collective-permute-start | bytes 129032 | tf_op jit(solution)/shard_map/ppermute | solution.py:531
  21.3 5.3 %collective-permute-start.8 = (bf16[168,128]{1,0:T(8,128)(2,1)S(1)}, bf16[168,128]{1,0:T(8,128)(2,1)S(1)}, u32[]{:S(2)}, u32[]{:S(2)}) collective-permute-start(bf16[168,128]{1,0:T(8,128)(2,1)S(1)} %get-tuple-element.12), channel_id=1, source_target_pairs={{0,6},{1,7},{2,4},{3,5},{4,2},{5,3},{6,0},{7,1},{8,14},{9,15},{10,... | collective-permute-start | bytes 129032 | tf_op jit(solution)/shard_map/ppermute | solution.py:531
  22.0 4.7 %collective-permute-start.7 = (bf16[168,128]{1,0:T(8,128)(2,1)S(1)}, bf16[168,128]{1,0:T(8,128)(2,1)S(1)}, u32[]{:S(2)}, u32[]{:S(2)}) collective-permute-start(bf16[168,128]{1,0:T(8,128)(2,1)S(1)} %get-tuple-element.13), channel_id=1, source_target_pairs={{0,5},{1,4},{2,7},{3,6},{4,1},{5,0},{6,3},{7,2},{8,13},{9,12},{10,... | collective-permute-start | bytes 129032 | tf_op jit(solution)/shard_map/ppermute | solution.py:531
  23.4 4.4 %collective-permute-start.6 = (bf16[168,128]{1,0:T(8,128)(2,1)S(1)}, bf16[168,128]{1,0:T(8,128)(2,1)S(1)}, u32[]{:S(2)}, u32[]{:S(2)}) collective-permute-start(bf16[168,128]{1,0:T(8,128)(2,1)S(1)} %get-tuple-element.14), channel_id=1, source_target_pairs={{0,4},{1,5},{2,6},{3,7},{4,0},{5,1},{6,2},{7,3},{8,12},{9,13},{10,... | collective-permute-start | bytes 129032 | tf_op jit(solution)/shard_map/ppermute | solution.py:531
  23.9 3.9 %collective-permute-start.5 = (bf16[168,128]{1,0:T(8,128)(2,1)S(1)}, bf16[168,128]{1,0:T(8,128)(2,1)S(1)}, u32[]{:S(2)}, u32[]{:S(2)}) collective-permute-start(bf16[168,128]{1,0:T(8,128)(2,1)S(1)} %get-tuple-element.15), channel_id=1, source_target_pairs={{0,3},{1,2},{2,1},{3,0},{4,7},{5,6},{6,5},{7,4},{8,11},{9,10},{10,... | collective-permute-start | bytes 129032 | tf_op jit(solution)/shard_map/ppermute | solution.py:531
  24.7 4.3 %collective-permute-start.4 = (bf16[168,128]{1,0:T(8,128)(2,1)S(1)}, bf16[168,128]{1,0:T(8,128)(2,1)S(1)}, u32[]{:S(2)}, u32[]{:S(2)}) collective-permute-start(bf16[168,128]{1,0:T(8,128)(2,1)S(1)} %get-tuple-element.16), channel_id=1, source_target_pairs={{0,2},{1,3},{2,0},{3,1},{4,6},{5,7},{6,4},{7,5},{8,10},{9,11},{10,... | collective-permute-start | bytes 129032 | tf_op jit(solution)/shard_map/ppermute | solution.py:531
  26.6 2.4 %collective-permute-start.3 = (bf16[168,128]{1,0:T(8,128)(2,1)S(1)}, bf16[168,128]{1,0:T(8,128)(2,1)S(1)}, u32[]{:S(2)}, u32[]{:S(2)}) collective-permute-start(bf16[168,128]{1,0:T(8,128)(2,1)S(1)} %get-tuple-element.17), channel_id=1, source_target_pairs={{0,1},{1,0},{2,3},{3,2},{4,5},{5,4},{6,7},{7,6},{8,9},{9,8},{10,11... | collective-permute-start | bytes 129032 | tf_op jit(solution)/shard_map/ppermute | solution.py:531
  30.3 7.2 %collective-permute-start.12 = (bf16[328,128]{1,0:T(8,128)(2,1)S(1)}, bf16[328,128]{1,0:T(8,128)(2,1)S(1)}, u32[]{:S(2)}, u32[]{:S(2)}) collective-permute-start(bf16[328,128]{1,0:T(8,128)(2,1)S(1)} %get-tuple-element.19), channel_id=1, source_target_pairs={{0,24},{8,16},{16,8},{24,0},{1,25},{9,17},{17,9},{25,1},{2,26},{10... | collective-permute-start | bytes 251912 | tf_op jit(solution)/shard_map/ppermute | solution.py:531
  32.9 7.2 %collective-permute-start.11 = (bf16[328,128]{1,0:T(8,128)(2,1)S(1)}, bf16[328,128]{1,0:T(8,128)(2,1)S(1)}, u32[]{:S(2)}, u32[]{:S(2)}) collective-permute-start(bf16[328,128]{1,0:T(8,128)(2,1)S(1)} %get-tuple-element.20), channel_id=1, source_target_pairs={{0,16},{8,24},{16,0},{24,8},{1,17},{9,25},{17,1},{25,9},{2,18},{10... | collective-permute-start | bytes 251912 | tf_op jit(solution)/shard_map/ppermute | solution.py:531
  32.9 7.2 %copy-start.1 = (bf16[256,256]{1,0:T(8,128)(2,1)S(1)}, bf16[256,256]{1,0:T(8,128)(2,1)}, u32[]{:S(2)}) copy-start(bf16[256,256]{1,0:T(8,128)(2,1)} %constant.104.clone.refs_4_) | copy-start | bytes 393220
  32.9 7.2 %copy-start.2 = (bf16[144,144]{1,0:T(8,128)(2,1)S(1)}, bf16[144,144]{1,0:T(8,128)(2,1)}, u32[]{:S(2)}) copy-start(bf16[144,144]{1,0:T(8,128)(2,1)} %constant.105.clone.refs_5_) | copy-start | bytes 124420
  32.9 7.2 %collective-permute-start.10 = (bf16[328,128]{1,0:T(8,128)(2,1)S(1)}, bf16[328,128]{1,0:T(8,128)(2,1)S(1)}, u32[]{:S(2)}, u32[]{:S(2)}) collective-permute-start(bf16[328,128]{1,0:T(8,128)(2,1)S(1)} %get-tuple-element.21), channel_id=1, source_target_pairs={{0,8},{8,0},{16,24},{24,16},{1,9},{9,1},{17,25},{25,17},{2,10},{10... | collective-permute-start | bytes 251912 | tf_op jit(solution)/shard_map/ppermute | solution.py:531
where the time goes:
time: 42.4 us; the launch traced here: 42.1 us
  starting transfers between devices  16.6 us (39%)
  waiting for transfers between devices  13 us (31%)
  Pallas kernels  11.3 us (27%)
  local copies, waits for them, and re-layouts  1.06 us (2%)
    ppermute x13, starting transfers between devices, exchange(): slab = lax.ppermute(slab, axis, [(n, n ^ s) for n in range(size)])  16.6 us
    ppermute x13, waiting for transfers between devices, exchange(): slab = lax.ppermute(slab, axis, [(n, n ^ s) for n in range(size)])  13 us
    pallas_call x1, Pallas kernels, packed(): pl.pallas_call(functools.partial(far_kernel, plan, depth), out_shape=(plt...  2.89 us
    pallas_call x1, Pallas kernels, packed(): pl.pallas_call(functools.partial(near_kernel, plan, depth), out_shape=plt...  2.41 us
    pallas_call x1, Pallas kernels, fetch(): pl.pallas_call(fetch_kernel, out_shape=pltpu.VMEM(w_out.shape, w_out.dtyp...  2.34 us
    pallas_call x1, Pallas kernels, packed(): pl.pallas_call(functools.partial(tail_kernel, plan), out_shape=jax.ShapeD...  2.08 us
    pallas_call x1, Pallas kernels, packed(): pl.pallas_call(functools.partial(second_kernel, plan, scaling), out_shape...  1.24 us
    squeeze x1, local copies, waits for them, and re-layouts, packed(): lax.dynamic_index_in_dim(jnp.asarray(first_tables(plan), half_type), col,...  0.92 us
  transfers between devices with their start and end apart: 13, of which 7 were waited for; matrix products, arithmetic and copies ran while one was open for 2% of the time, Pallas kernels for 6%

commit v1 on v0

--- a/solution.py
+++ b/solution.py
@@ -124,7 +124,8 @@
 
 LANES = 128
 TILE = 8
-STEPS = 2
+STEPS = 1
+WIDE = 256
 VMEM = pl.BlockSpec(memory_space=pltpu.VMEM)
 HBM = pl.BlockSpec(memory_space=pltpu.HBM)
 
@@ -168,7 +169,7 @@
             and self.length_first == 4 * self.cols
             and self.length_second % self.rows == 0
             and 2 * self.block_b % TILE == 0
-            and self.features % 256 == 0
+            and self.features % 512 == 0
         )
 
 
@@ -453,43 +454,73 @@
     place = jnp.where(last, lane - plan.full * LANES + row * sub, lane & (LANES - 1))
     is_sine = place > GROUP // 2
     span = 2 * plan.block_b
-    kept = {}
+    total = plan.rows * span
+    tails = {}
     for i in range(plan.pairs):
         table = first_ref if i == 0 else usual_ref
-        values = rhs_ref[i]
+        both = dot(table[...], rhs_ref[i])
         for r in range(plan.rows):
-            cosine = dot(table[0, r * span : (r + 1) * span, :], values)
-            sine = dot(table[1, r * span : (r + 1) * span, :], values)
+            cosine, sine = both[r * span : (r + 1) * span, :], both[total + r * span : total + (r + 1) * span, :]
             merged = jnp.where(is_sine, sine, cosine) * scaling
             for f in range(plan.full):
                 at = f * plan.out_rows + i * span
                 out_ref[r, at : at + span, :] = merged[:, f * LANES : (f + 1) * LANES].astype(jnp.bfloat16)
-            tail = merged[:, plan.full * LANES :]
-            for t in range(span // TILE):
-                whole, inner = divmod(i * (span // TILE) + t, plan.rows)
-                at = plan.full * plan.out_rows + whole * TILE
-                piece = turn_lanes(tail[t * TILE : (t + 1) * TILE, :], inner * sub)
-                if inner:
-                    piece = jnp.where(lane_index(piece.shape) >= inner * sub, piece, kept[r])
-                kept[r] = piece
-                if inner == plan.rows - 1 or (i == plan.pairs - 1 and t == span // TILE - 1):
-                    out_ref[r, at : at + TILE, :] = piece.astype(jnp.bfloat16)
+            tails[i, r] = merged[:, plan.full * LANES :]
+    for r in range(plan.rows):
+        pieces = []
+        for t in range(plan.row_tiles):
+            i, at = divmod(t * TILE, span)
+            pieces.append(turn_lanes(tails[i, r][at : at + TILE, :], (t % plan.rows) * sub))
+        for whole in range(plan.back_quads):
+            at = plan.full * plan.out_rows + whole * TILE
+            group = pieces[whole * plan.rows : (whole + 1) * plan.rows]
+            out_ref[r, at : at + TILE, :] = by_lane(group, sub).astype(jnp.bfloat16)
+
+
+def unfolded(plan, order, unfold, slabs):
+    pair = [slabs[f * plan.out_rows : (f + 1) * plan.out_rows, :] for f in range(plan.full)]
+    ordered = dot(order, jnp.concatenate(pair, axis=1)).astype(jnp.bfloat16)
+    return dot(ordered, unfold).astype(jnp.bfloat16)
+
+
+def early_kernel(plan, slab_ref, unfold_ref, order_ref, w_hbm, partial_ref, w_ref, own_ref, sems):
+    row = lax.axis_index("row")
+    each = plan.full * GROUP
+
+    def part(s):
+        return w_hbm.at[pl.ds(pl.multiple_of((row ^ s) * each, LANES), each), :]
+
+    copies = [pltpu.make_async_copy(part(0), own_ref, sems.at[0])]
+    for s in range(1, plan.rows):
+        copies.append(pltpu.make_async_copy(part(s), w_ref.at[pl.ds((s - 1) * each, each), :], sems.at[s]))
+    copies.append(
+        pltpu.make_async_copy(
+            w_hbm.at[pl.ds(plan.rows * each, GROUP), :],
+            w_ref.at[pl.ds((plan.rows - 1) * each, GROUP), :],
+            sems.at[plan.rows],
+        )
+    )
+    for copy in copies:
+        copy.start()
+    spectrum = unfolded(plan, order_ref[...], unfold_ref[...], slab_ref)
+    copies[0].wait()
+    for n in range(plan.features // WIDE):
+        columns = slice(n * WIDE, (n + 1) * WIDE)
+        partial_ref[:, columns] = dot(spectrum, own_ref[:, columns])
+    for copy in copies[1:]:
+        copy.wait()
 
 
 def tail_kernel(plan, *refs):
     slabs = refs[: plan.rows]
-    unfold_ref, order_ref, w_ref, out_ref, held_ref, spectrum_ref = refs[plan.rows :]
+    unfold_ref, order_ref, partial_ref, w_ref, out_hbm, packed_ref, stage_ref, sems = refs[plan.rows :]
     row = lax.axis_index("row")
+    main = plan.full * plan.out_rows
     for s in range(plan.rows):
-        held_ref[row ^ s] = slabs[s][...]
-    order = order_ref[...]
-    unfold = unfold_ref[...]
-    for q in range(plan.rows):
-        pair = [held_ref[q, f * plan.out_rows : (f + 1) * plan.out_rows, :] for f in range(plan.full)]
-        ordered = dot(order, jnp.concatenate(pair, axis=1)).astype(jnp.bfloat16)
-        spectrum_ref[:, q * 2 * GROUP : (q + 1) * 2 * GROUP] = dot(ordered, unfold).astype(jnp.bfloat16)
-    base = plan.full * plan.out_rows
-    packed = [held_ref[q, base:, :].astype(jnp.float32) for q in range(plan.rows)]
+        packed_ref[row ^ s] = slabs[s][main:, :]
+    order, unfold = order_ref[...], unfold_ref[...]
+    spectrum = [unfolded(plan, order, unfold, slabs[s]) for s in range(1, plan.rows)]
+    packed = [packed_ref[q].astype(jnp.float32) for q in range(plan.rows)]
     turned = [[turn_lanes(value, plan.sub * t) for t in range(plan.rows)] for value in packed]
     pieces = []
     for t in range(plan.row_tiles):
@@ -500,14 +531,20 @@
         )
     last = jnp.concatenate(pieces, axis=0).astype(jnp.bfloat16)
     ordered = dot(order, last).astype(jnp.bfloat16)
-    spectrum_ref[:, plan.rows * 2 * GROUP :] = dot(ordered, unfold[:GROUP, :GROUP]).astype(jnp.bfloat16)
-    wide = 256
+    spectrum.append(dot(ordered, unfold[:GROUP, :GROUP]).astype(jnp.bfloat16))
+    spectrum = jnp.concatenate(spectrum, axis=1)
     group = 2 * plan.pairs
-    for n in range(plan.features // wide):
-        columns = slice(n * wide, (n + 1) * wide)
-        result = dot(spectrum_ref[...], w_ref[:, columns]).astype(jnp.bfloat16)
+    copies = []
+    for n in range(plan.features // WIDE):
+        columns = slice(n * WIDE, (n + 1) * WIDE)
+        result = (partial_ref[:, columns] + dot(spectrum, w_ref[:, columns])).astype(jnp.bfloat16)
         for k in range(plan.block_b):
-            out_ref[k, :, columns] = result[k * group : (k + 1) * group, :]
+            stage_ref[n, k] = result[k * group : (k + 1) * group, :]
+        copy = pltpu.make_async_copy(stage_ref.at[n], out_hbm.at[:, :, pl.ds(n * WIDE, WIDE)], sems.at[n])
+        copy.start()
+        copies.append(copy)
+    for copy in copies:
+        copy.wait()
 
 
 def estimate(flops, moved):
@@ -531,25 +568,6 @@
             slab = lax.ppermute(slab, axis, [(n, n ^ s) for n in range(size)])
         out.append(slab)
     return out
-
-
-def fetch_kernel(w_hbm, after_ref, w_ref, sem):
-    copy = pltpu.make_async_copy(w_hbm, w_ref, sem)
-    copy.start()
-    copy.wait()
-
-
-def fetch(w_out, after):
-    return pl.pallas_call(
-        fetch_kernel,
-        out_shape=pltpu.VMEM(w_out.shape, w_out.dtype),
-        in_specs=[HBM, VMEM],
-        out_specs=VMEM,
-        scratch_shapes=[pltpu.SemaphoreType.DMA],
-        compiler_params=limit(2),
-        cost_estimate=estimate(10**9, 2 * w_out.size),
-        name="fetch",
-    )(pltpu.with_memory_space_constraint(w_out, pltpu.HBM), after)
 
 
 def packed(plan, tokens, norm_gain, w_in, w_out):
@@ -613,6 +631,7 @@
     )(*slabs, first)
     slabs = exchange(turned, "col", plan.cols)
     usual, special = (jnp.asarray(table, half_type) for table in second_tables(plan))
+    usual, special = (table.reshape(-1, table.shape[-1]) for table in (usual, special))
     leading = jnp.where(col == 0, special, usual)
     depth = plan.half * plan.cols * 4
     back = pl.pallas_call(
@@ -629,20 +648,37 @@
         name="second",
     )(*slabs, usual, leading)
     slabs = exchange(back, "row", plan.rows)
-    w_out = fetch(w_out, slabs[0][:TILE])
+    unfold = jnp.asarray(paired(unfold_table()), half_type)
+    order = jnp.asarray(order_table(plan), half_type)
+    main, each = plan.full * plan.out_rows, plan.full * GROUP
+    cost = estimate(local * features * channels, features * channels)
+    partial, w_rest = pl.pallas_call(
+        functools.partial(early_kernel, plan),
+        out_shape=(
+            pltpu.VMEM((plan.out_rows, features), jnp.float32),
+            pltpu.VMEM((channels - each, features), half_type),
+        ),
+        in_specs=[VMEM] * 3 + [HBM],
+        out_specs=(VMEM, VMEM),
+        scratch_shapes=[pltpu.VMEM((each, features), half_type), pltpu.SemaphoreType.DMA((plan.rows + 1,))],
+        compiler_params=limit(8),
+        cost_estimate=cost,
+        name="early",
+    )(slabs[0], unfold, order, pltpu.with_memory_space_constraint(w_out, pltpu.HBM))
     return pl.pallas_call(
         functools.partial(tail_kernel, plan),
         out_shape=jax.ShapeDtypeStruct((plan.block_b, 2 * plan.pairs, features), half_type),
-        in_specs=[VMEM] * (plan.rows + 3),
-        out_specs=VMEM,
+        in_specs=[VMEM] * (plan.rows + 4),
+        out_specs=HBM,
         scratch_shapes=[
-            pltpu.VMEM((plan.rows, plan.back_rows, LANES), half_type),
-            pltpu.VMEM((plan.out_rows, channels), half_type),
+            pltpu.VMEM((plan.rows, plan.back_rows - main, LANES), half_type),
+            pltpu.VMEM((features // WIDE, plan.block_b, 2 * plan.pairs, WIDE), half_type),
+            pltpu.SemaphoreType.DMA((features // WIDE,)),
         ],
         compiler_params=limit(12),
-        cost_estimate=estimate(2 * local * features * channels, 2 * features * channels),
+        cost_estimate=cost,
         name="tail",
-    )(*slabs, jnp.asarray(paired(unfold_table()), half_type), jnp.asarray(order_table(plan), half_type), w_out)
+    )(*slabs, unfold, order, partial, w_rest)
 
 
 def shards(tokens, norm_gain, w_in, w_out):

time: 42.4 us -> 41.7 us (0.983)
  Pallas kernels: 11.3 us -> 10.6 us
where the time goes in v1:
time: 41.7 us; the launch traced here: 41.5 us
  starting transfers between devices  16.6 us (40%)
  waiting for transfers between devices  13 us (31%)
  Pallas kernels  10.6 us (25%)
  local copies, waits for them, and re-layouts  1.07 us (3%)
    ppermute x13, starting transfers between devices, exchange(): slab = lax.ppermute(slab, axis, [(n, n ^ s) for n in range(size)])  16.6 us
    ppermute x13, waiting for transfers between devices, exchange(): slab = lax.ppermute(slab, axis, [(n, n ^ s) for n in range(size)])  13 us
    pallas_call x1, Pallas kernels, packed(): pl.pallas_call(functools.partial(far_kernel, plan, depth), out_shape=(plt...  2.88 us
    pallas_call x1, Pallas kernels, packed(): pl.pallas_call(functools.partial(near_kernel, plan, depth), out_shape=plt...  2.43 us
    pallas_call x1, Pallas kernels, packed(): pl.pallas_call(functools.partial(early_kernel, plan), out_shape=(pltpu.VM...  2.37 us
    pallas_call x1, Pallas kernels, packed(): pl.pallas_call(functools.partial(tail_kernel, plan), out_shape=jax.ShapeD...  1.74 us
    squeeze x1, local copies, waits for them, and re-layouts, packed(): lax.dynamic_index_in_dim(jnp.asarray(first_tables(plan), half_type), col,...  0.92 us
    pallas_call x1, Pallas kernels, packed(): pl.pallas_call(functools.partial(second_kernel, plan, scaling), out_shape...  0.87 us
  transfers between devices with their start and end apart: 13, of which 7 were waited for; matrix products, arithmetic and copies ran while one was open for 2% of the time, Pallas kernels for 6%

profile of v1, /device:TPU:0, one launch (start us, length us, event | category | flops | bytes accessed | tf_op | source)
XLA Modules:
  0.0 41.5 jit_solution(2675835011910927306)
XLA Ops:
  0.0 2.9 %far.1 = (bf16[2,336,128]{2,1,0:T(8,128)(2,1)S(1)}, bf16[2,48,128]{2,1,0:T(8,128)(2,1)S(1)}, bf16[144,2048]{1,0:T(8,128)(2,1)S(1)}) custom-call(bf16[144,2048]{1,0:T(8,128)(2,1)} %bitcast.38, bf16[16,128]{1,0:T(8,128)(2,1)} %bitcast.39, bf16[2048,1152]{1,0:T(8,128)(2,1)} %w_hbm.4, bf16[256,256]{1,0:T(8,128)(2,1)} %constant.100.clone.table_hbm), custom_call_target="tpu_custom_call" | custom-call | flops 339738624 | bytes 2359296 | tf_op jit(solution)/shard_map/far/pallas_call | solution.py:584
  2.9 0.0 copy-start
  2.9 0.0 copy-start.3
  2.9 2.4 %near.1 = bf16[2,336,128]{2,1,0:T(8,128)(2,1)S(1)} custom-call(bf16[144,2048]{1,0:T(8,128)(2,1)S(1)} %get-tuple-element.10.normed_ref, bf16[2,48,128]{2,1,0:T(8,128)(2,1)S(1)} %get-tuple-element.11.near_ref, bf16[2048,1152]{1,0:T(8,128)(2,1)} %w_hbm.4, bf16[256,256]{1,0:T(8,128)(2,1)} %constant.100.clone.table_hbm), custom_call_target="tpu_custom_call" | custom-call | flops 339738624 | bytes 2359296 | tf_op jit(solution)/shard_map/near/pallas_call | solution.py:605
  5.3 0.0 copy-start.1
  5.4 0.0 copy-start.2
  5.4 3.1 %collective-permute-start = (bf16[336,128]{1,0:T(8,128)(2,1)S(1)}, bf16[336,128]{1,0:T(8,128)(2,1)S(1)}, u32[]{:S(2)}, u32[]{:S(2)}) collective-permute-start(bf16[336,128]{1,0:T(8,128)(2,1)S(1)} %get-tuple-element.29), channel_id=1, source_target_pairs={{0,8},{8,0},{16,24},{24,16},{1,9},{9,1},{17,25},{25,17},{2,10},{10... | collective-permute-start | bytes 258056 | tf_op jit(solution)/shard_map/ppermute | solution.py:568
  8.5 2.5 %collective-permute-start.2 = (bf16[336,128]{1,0:T(8,128)(2,1)S(1)}, bf16[336,128]{1,0:T(8,128)(2,1)S(1)}, u32[]{:S(2)}, u32[]{:S(2)}) collective-permute-start(bf16[336,128]{1,0:T(8,128)(2,1)S(1)} %get-tuple-element.27), channel_id=1, source_target_pairs={{0,24},{8,16},{16,8},{24,0},{1,25},{9,17},{17,9},{25,1},{2,26},{10... | collective-permute-start | bytes 258056 | tf_op jit(solution)/shard_map/ppermute | solution.py:568
  11.1 0.2 collective-permute-start.1
  11.3 0.9 %dynamic-slice_bitcast_fusion.refs_4_ = bf16[9,64,64]{2,1,0:T(8,128)(2,1)S(1)} fusion(bf16[8,9,64,64]{3,2,1,0:T(8,128)(2,1)} %constant.101.clone, s32[]{:T(128)S(6)} %select_n.88), kind=kLoop, calls=%fused_computation.1 | loop fusion | bytes 147460 | tf_op jit(solution)/shard_map/jit(dynamic_index_in_dim)/squeeze | solution.py:621
  12.2 0.0 collective-permute-done.refs_1_
  12.2 4.1 %collective-permute-done.2.refs_3_ = bf16[336,128]{1,0:T(8,128)(2,1)S(1)} collective-permute-done((bf16[336,128]{1,0:T(8,128)(2,1)S(1)}, bf16[336,128]{1,0:T(8,128)(2,1)S(1)}, u32[]{:S(2)}, u32[]{:S(2)}) %collective-permute-start.2) | collective-permute-done | bytes 86048 | tf_op jit(solution)/shard_map/ppermute | solution.py:568
  16.3 2.8 %collective-permute-done.1.refs_2_ = bf16[336,128]{1,0:T(8,128)(2,1)S(1)} collective-permute-done((bf16[336,128]{1,0:T(8,128)(2,1)S(1)}, bf16[336,128]{1,0:T(8,128)(2,1)S(1)}, u32[]{:S(2)}, u32[]{:S(2)}) %collective-permute-start.1) | collective-permute-done | bytes 86048 | tf_op jit(solution)/shard_map/ppermute | solution.py:568
  19.1 0.3 first.1
  19.5 1.9 %collective-permute-start.9 = (bf16[168,128]{1,0:T(8,128)(2,1)S(1)}, bf16[168,128]{1,0:T(8,128)(2,1)S(1)}, u32[]{:S(2)}, u32[]{:S(2)}) collective-permute-start(bf16[168,128]{1,0:T(8,128)(2,1)S(1)} %get-tuple-element.15), channel_id=1, source_target_pairs={{0,7},{1,6},{2,5},{3,4},{4,3},{5,2},{6,1},{7,0},{8,15},{9,14},{10,... | collective-permute-start | bytes 129032 | tf_op jit(solution)/shard_map/ppermute | solution.py:568
  21.3 0.7 %collective-permute-start.8 = (bf16[168,128]{1,0:T(8,128)(2,1)S(1)}, bf16[168,128]{1,0:T(8,128)(2,1)S(1)}, u32[]{:S(2)}, u32[]{:S(2)}) collective-permute-start(bf16[168,128]{1,0:T(8,128)(2,1)S(1)} %get-tuple-element.16), channel_id=1, source_target_pairs={{0,6},{1,7},{2,4},{3,5},{4,2},{5,3},{6,0},{7,1},{8,14},{9,15},{10,... | collective-permute-start | bytes 129032 | tf_op jit(solution)/shard_map/ppermute | solution.py:568
  22.1 1.4 %collective-permute-start.7 = (bf16[168,128]{1,0:T(8,128)(2,1)S(1)}, bf16[168,128]{1,0:T(8,128)(2,1)S(1)}, u32[]{:S(2)}, u32[]{:S(2)}) collective-permute-start(bf16[168,128]{1,0:T(8,128)(2,1)S(1)} %get-tuple-element.17), channel_id=1, source_target_pairs={{0,5},{1,4},{2,7},{3,6},{4,1},{5,0},{6,3},{7,2},{8,13},{9,12},{10,... | collective-permute-start | bytes 129032 | tf_op jit(solution)/shard_map/ppermute | solution.py:568
  23.4 0.5 %collective-permute-start.6 = (bf16[168,128]{1,0:T(8,128)(2,1)S(1)}, bf16[168,128]{1,0:T(8,128)(2,1)S(1)}, u32[]{:S(2)}, u32[]{:S(2)}) collective-permute-start(bf16[168,128]{1,0:T(8,128)(2,1)S(1)} %get-tuple-element.18), channel_id=1, source_target_pairs={{0,4},{1,5},{2,6},{3,7},{4,0},{5,1},{6,2},{7,3},{8,12},{9,13},{10,... | collective-permute-start | bytes 129032 | tf_op jit(solution)/shard_map/ppermute | solution.py:568
  23.9 0.8 %collective-permute-start.5 = (bf16[168,128]{1,0:T(8,128)(2,1)S(1)}, bf16[168,128]{1,0:T(8,128)(2,1)S(1)}, u32[]{:S(2)}, u32[]{:S(2)}) collective-permute-start(bf16[168,128]{1,0:T(8,128)(2,1)S(1)} %get-tuple-element.19), channel_id=1, source_target_pairs={{0,3},{1,2},{2,1},{3,0},{4,7},{5,6},{6,5},{7,4},{8,11},{9,10},{10,... | collective-permute-start | bytes 129032 | tf_op jit(solution)/shard_map/ppermute | solution.py:568
  24.8 0.0 collective-permute-done.9.refs_7_
  24.8 1.0 %collective-permute-start.4 = (bf16[168,128]{1,0:T(8,128)(2,1)S(1)}, bf16[168,128]{1,0:T(8,128)(2,1)S(1)}, u32[]{:S(2)}, u32[]{:S(2)}) collective-permute-start(bf16[168,128]{1,0:T(8,128)(2,1)S(1)} %get-tuple-element.20), channel_id=1, source_target_pairs={{0,2},{1,3},{2,0},{3,1},{4,6},{5,7},{6,4},{7,5},{8,10},{9,11},{10,... | collective-permute-start | bytes 129032 | tf_op jit(solution)/shard_map/ppermute | solution.py:568
  25.8 0.9 %collective-permute-done.8.refs_6_ = bf16[168,128]{1,0:T(8,128)(2,1)S(1)} collective-permute-done((bf16[168,128]{1,0:T(8,128)(2,1)S(1)}, bf16[168,128]{1,0:T(8,128)(2,1)S(1)}, u32[]{:S(2)}, u32[]{:S(2)}) %collective-permute-start.8) | collective-permute-done | bytes 43040 | tf_op jit(solution)/shard_map/ppermute | solution.py:568
  26.6 0.1 broadcast_select_fusion.refs_9_
  26.7 1.1 %collective-permute-done.6.refs_4_ = bf16[168,128]{1,0:T(8,128)(2,1)S(1)} collective-permute-done((bf16[168,128]{1,0:T(8,128)(2,1)S(1)}, bf16[168,128]{1,0:T(8,128)(2,1)S(1)}, u32[]{:S(2)}, u32[]{:S(2)}) %collective-permute-start.6) | collective-permute-done | bytes 43040 | tf_op jit(solution)/shard_map/ppermute | solution.py:568
  27.8 1.2 %collective-permute-done.4.refs_2_ = bf16[168,128]{1,0:T(8,128)(2,1)S(1)} collective-permute-done((bf16[168,128]{1,0:T(8,128)(2,1)S(1)}, bf16[168,128]{1,0:T(8,128)(2,1)S(1)}, u32[]{:S(2)}, u32[]{:S(2)}) %collective-permute-start.4) | collective-permute-done | bytes 43040 | tf_op jit(solution)/shard_map/ppermute | solution.py:568
  29.0 0.9 %second.1 = bf16[4,328,128]{2,1,0:T(8,128)(2,1)S(1)} custom-call(bf16[168,128]{1,0:T(8,128)(2,1)S(1)} %get-tuple-element.22.refs_0_, bf16[168,128]{1,0:T(8,128)(2,1)S(1)} %collective-permute-done.3.refs_1_, bf16[168,128]{1,0:T(8,128)(2,1)S(1)} %collective-permute-done.4.refs_2_, bf16[168,128]{1,0:T(8,128)(2,1)S(1)} %collective-permute-done.5.refs_3_, ...), custom_call_target="tpu_custom_call" | custom-call | flops 300000000 | bytes 1000000 | tf_op jit(solution)/shard_map/second/pallas_call | solution.py:637
  30.0 2.6 %collective-permute-start.12 = (bf16[328,128]{1,0:T(8,128)(2,1)S(1)}, bf16[328,128]{1,0:T(8,128)(2,1)S(1)}, u32[]{:S(2)}, u32[]{:S(2)}) collective-permute-start(bf16[328,128]{1,0:T(8,128)(2,1)S(1)} %get-tuple-element.23), channel_id=1, source_target_pairs={{0,24},{8,16},{16,8},{24,0},{1,25},{9,17},{17,9},{25,1},{2,26},{10... | collective-permute-start | bytes 251912 | tf_op jit(solution)/shard_map/ppermute | solution.py:568
  32.6 1.9 %collective-permute-start.10 = (bf16[328,128]{1,0:T(8,128)(2,1)S(1)}, bf16[328,128]{1,0:T(8,128)(2,1)S(1)}, u32[]{:S(2)}, u32[]{:S(2)}) collective-permute-start(bf16[328,128]{1,0:T(8,128)(2,1)S(1)} %get-tuple-element.25), channel_id=1, source_target_pairs={{0,8},{8,0},{16,24},{24,16},{1,9},{9,1},{17,25},{25,17},{2,10},{10... | collective-permute-start | bytes 251912 | tf_op jit(solution)/shard_map/ppermute | solution.py:568
  34.4 2.4 %early.1 = (f32[144,2048]{1,0:T(8,128)S(1)}, bf16[896,2048]{1,0:T(8,128)(2,1)S(1)}) custom-call(bf16[328,128]{1,0:T(8,128)(2,1)S(1)} %get-tuple-element.26.slab_ref.refs_0_, bf16[256,256]{1,0:T(8,128)(2,1)S(1)} %copy-done.1, bf16[144,144]{1,0:T(8,128)(2,1)S(1)} %copy-done.2, bf16[1152,2048]{1,0:T(8,128)(2,1)} %w_hbm.5), custom_call_target="tpu_custom_call" | custom-call | flops 339738624 | bytes 2359296 | tf_op jit(solution)/shard_map/early/pallas_call | solution.py:655
  36.8 0.3 collective-permute-done.12.refs_3_
  37.1 2.6 %collective-permute-done.11.refs_2_ = bf16[328,128]{1,0:T(8,128)(2,1)S(1)} collective-permute-done((bf16[328,128]{1,0:T(8,128)(2,1)S(1)}, bf16[328,128]{1,0:T(8,128)(2,1)S(1)}, u32[]{:S(2)}, u32[]{:S(2)}) %collective-permute-start.11) | collective-permute-done | bytes 84000 | tf_op jit(solution)/shard_map/ppermute | solution.py:568
  39.7 1.7 %tail.1 = bf16[36,4,2048]{2,1,0:T(4,128)(2,1)} custom-call(bf16[328,128]{1,0:T(8,128)(2,1)S(1)} %get-tuple-element.26.slab_ref.refs_0_, bf16[328,128]{1,0:T(8,128)(2,1)S(1)} %collective-permute-done.10.refs_1_, bf16[328,128]{1,0:T(8,128)(2,1)S(1)} %collective-permute-done.11.refs_2_, bf16[328,128]{1,0:T(8,128)(2,1)S(1)} %collective-permute-done.12.refs_3_, ...), custom_call_target="tpu_custom_call" | custom-call | flops 339738624 | bytes 2359296 | tf_op jit(solution)/shard_map/tail/pallas_call | solution.py:668
  (14 shorter events, 0.1 us)
Async XLA Ops:
  2.9 23.7 %copy-start = (bf16[576,288]{1,0:T(8,128)(2,1)S(1)}, bf16[576,288]{1,0:T(8,128)(2,1)}, u32[]{:S(2)}) copy-start(bf16[576,288]{1,0:T(8,128)(2,1)} %constant.107.refs_8_) | copy-start | bytes 995332
  2.9 23.7 %copy-start.3 = (bf16[576,288]{1,0:T(8,128)(2,1)S(1)}, bf16[576,288]{1,0:T(8,128)(2,1)}, u32[]{:S(2)}) copy-start(bf16[576,288]{1,0:T(8,128)(2,1)} %constant.108) | copy-start | bytes 995332
  5.3 29.1 %copy-start.1 = (bf16[256,256]{1,0:T(8,128)(2,1)S(1)}, bf16[256,256]{1,0:T(8,128)(2,1)}, u32[]{:S(2)}) copy-start(bf16[256,256]{1,0:T(8,128)(2,1)} %constant.104.clone.unfold_ref.refs_4_) | copy-start | bytes 393220
  5.4 29.1 %copy-start.2 = (bf16[144,144]{1,0:T(8,128)(2,1)S(1)}, bf16[144,144]{1,0:T(8,128)(2,1)}, u32[]{:S(2)}) copy-start(bf16[144,144]{1,0:T(8,128)(2,1)} %constant.105.clone.order_ref.refs_5_) | copy-start | bytes 124420
  5.4 6.8 %collective-permute-start = (bf16[336,128]{1,0:T(8,128)(2,1)S(1)}, bf16[336,128]{1,0:T(8,128)(2,1)S(1)}, u32[]{:S(2)}, u32[]{:S(2)}) collective-permute-start(bf16[336,128]{1,0:T(8,128)(2,1)S(1)} %get-tuple-element.29), channel_id=1, source_target_pairs={{0,8},{8,0},{16,24},{24,16},{1,9},{9,1},{17,25},{25,17},{2,10},{10... | collective-permute-start | bytes 258056 | tf_op jit(solution)/shard_map/ppermute | solution.py:568
  8.5 7.8 %collective-permute-start.2 = (bf16[336,128]{1,0:T(8,128)(2,1)S(1)}, bf16[336,128]{1,0:T(8,128)(2,1)S(1)}, u32[]{:S(2)}, u32[]{:S(2)}) collective-permute-start(bf16[336,128]{1,0:T(8,128)(2,1)S(1)} %get-tuple-element.27), channel_id=1, source_target_pairs={{0,24},{8,16},{16,8},{24,0},{1,25},{9,17},{17,9},{25,1},{2,26},{10... | collective-permute-start | bytes 258056 | tf_op jit(solution)/shard_map/ppermute | solution.py:568
  11.1 8.0 %collective-permute-start.1 = (bf16[336,128]{1,0:T(8,128)(2,1)S(1)}, bf16[336,128]{1,0:T(8,128)(2,1)S(1)}, u32[]{:S(2)}, u32[]{:S(2)}) collective-permute-start(bf16[336,128]{1,0:T(8,128)(2,1)S(1)} %get-tuple-element.28), channel_id=1, source_target_pairs={{0,16},{8,24},{16,0},{24,8},{1,17},{9,25},{17,1},{25,9},{2,18},{10... | collective-permute-start | bytes 258056 | tf_op jit(solution)/shard_map/ppermute | solution.py:568
  19.5 5.3 %collective-permute-start.9 = (bf16[168,128]{1,0:T(8,128)(2,1)S(1)}, bf16[168,128]{1,0:T(8,128)(2,1)S(1)}, u32[]{:S(2)}, u32[]{:S(2)}) collective-permute-start(bf16[168,128]{1,0:T(8,128)(2,1)S(1)} %get-tuple-element.15), channel_id=1, source_target_pairs={{0,7},{1,6},{2,5},{3,4},{4,3},{5,2},{6,1},{7,0},{8,15},{9,14},{10,... | collective-permute-start | bytes 129032 | tf_op jit(solution)/shard_map/ppermute | solution.py:568
  21.3 5.3 %collective-permute-start.8 = (bf16[168,128]{1,0:T(8,128)(2,1)S(1)}, bf16[168,128]{1,0:T(8,128)(2,1)S(1)}, u32[]{:S(2)}, u32[]{:S(2)}) collective-permute-start(bf16[168,128]{1,0:T(8,128)(2,1)S(1)} %get-tuple-element.16), channel_id=1, source_target_pairs={{0,6},{1,7},{2,4},{3,5},{4,2},{5,3},{6,0},{7,1},{8,14},{9,15},{10,... | collective-permute-start | bytes 129032 | tf_op jit(solution)/shard_map/ppermute | solution.py:568
  22.1 4.7 %collective-permute-start.7 = (bf16[168,128]{1,0:T(8,128)(2,1)S(1)}, bf16[168,128]{1,0:T(8,128)(2,1)S(1)}, u32[]{:S(2)}, u32[]{:S(2)}) collective-permute-start(bf16[168,128]{1,0:T(8,128)(2,1)S(1)} %get-tuple-element.17), channel_id=1, source_target_pairs={{0,5},{1,4},{2,7},{3,6},{4,1},{5,0},{6,3},{7,2},{8,13},{9,12},{10,... | collective-permute-start | bytes 129032 | tf_op jit(solution)/shard_map/ppermute | solution.py:568
  23.4 4.4 %collective-permute-start.6 = (bf16[168,128]{1,0:T(8,128)(2,1)S(1)}, bf16[168,128]{1,0:T(8,128)(2,1)S(1)}, u32[]{:S(2)}, u32[]{:S(2)}) collective-permute-start(bf16[168,128]{1,0:T(8,128)(2,1)S(1)} %get-tuple-element.18), channel_id=1, source_target_pairs={{0,4},{1,5},{2,6},{3,7},{4,0},{5,1},{6,2},{7,3},{8,12},{9,13},{10,... | collective-permute-start | bytes 129032 | tf_op jit(solution)/shard_map/ppermute | solution.py:568
  23.9 3.9 %collective-permute-start.5 = (bf16[168,128]{1,0:T(8,128)(2,1)S(1)}, bf16[168,128]{1,0:T(8,128)(2,1)S(1)}, u32[]{:S(2)}, u32[]{:S(2)}) collective-permute-start(bf16[168,128]{1,0:T(8,128)(2,1)S(1)} %get-tuple-element.19), channel_id=1, source_target_pairs={{0,3},{1,2},{2,1},{3,0},{4,7},{5,6},{6,5},{7,4},{8,11},{9,10},{10,... | collective-permute-start | bytes 129032 | tf_op jit(solution)/shard_map/ppermute | solution.py:568
  24.8 4.3 %collective-permute-start.4 = (bf16[168,128]{1,0:T(8,128)(2,1)S(1)}, bf16[168,128]{1,0:T(8,128)(2,1)S(1)}, u32[]{:S(2)}, u32[]{:S(2)}) collective-permute-start(bf16[168,128]{1,0:T(8,128)(2,1)S(1)} %get-tuple-element.20), channel_id=1, source_target_pairs={{0,2},{1,3},{2,0},{3,1},{4,6},{5,7},{6,4},{7,5},{8,10},{9,11},{10,... | collective-permute-start | bytes 129032 | tf_op jit(solution)/shard_map/ppermute | solution.py:568
  26.6 2.4 %collective-permute-start.3 = (bf16[168,128]{1,0:T(8,128)(2,1)S(1)}, bf16[168,128]{1,0:T(8,128)(2,1)S(1)}, u32[]{:S(2)}, u32[]{:S(2)}) collective-permute-start(bf16[168,128]{1,0:T(8,128)(2,1)S(1)} %get-tuple-element.21), channel_id=1, source_target_pairs={{0,1},{1,0},{2,3},{3,2},{4,5},{5,4},{6,7},{7,6},{8,9},{9,8},{10,11... | collective-permute-start | bytes 129032 | tf_op jit(solution)/shard_map/ppermute | solution.py:568
  30.0 7.2 %collective-permute-start.12 = (bf16[328,128]{1,0:T(8,128)(2,1)S(1)}, bf16[328,128]{1,0:T(8,128)(2,1)S(1)}, u32[]{:S(2)}, u32[]{:S(2)}) collective-permute-start(bf16[328,128]{1,0:T(8,128)(2,1)S(1)} %get-tuple-element.23), channel_id=1, source_target_pairs={{0,24},{8,16},{16,8},{24,0},{1,25},{9,17},{17,9},{25,1},{2,26},{10... | collective-permute-start | bytes 251912 | tf_op jit(solution)/shard_map/ppermute | solution.py:568
  32.5 7.2 %collective-permute-start.11 = (bf16[328,128]{1,0:T(8,128)(2,1)S(1)}, bf16[328,128]{1,0:T(8,128)(2,1)S(1)}, u32[]{:S(2)}, u32[]{:S(2)}) collective-permute-start(bf16[328,128]{1,0:T(8,128)(2,1)S(1)} %get-tuple-element.24), channel_id=1, source_target_pairs={{0,16},{8,24},{16,0},{24,8},{1,17},{9,25},{17,1},{25,9},{2,18},{10... | collective-permute-start | bytes 251912 | tf_op jit(solution)/shard_map/ppermute | solution.py:568
  32.6 7.2 %collective-permute-start.10 = (bf16[328,128]{1,0:T(8,128)(2,1)S(1)}, bf16[328,128]{1,0:T(8,128)(2,1)S(1)}, u32[]{:S(2)}, u32[]{:S(2)}) collective-permute-start(bf16[328,128]{1,0:T(8,128)(2,1)S(1)} %get-tuple-element.25), channel_id=1, source_target_pairs={{0,8},{8,0},{16,24},{24,16},{1,9},{9,1},{17,25},{25,17},{2,10},{10... | collective-permute-start | bytes 251912 | tf_op jit(solution)/shard_map/ppermute | solution.py:568

commit v2 on v1

--- a/solution.py
+++ b/solution.py
@@ -126,6 +126,7 @@
 TILE = 8
 STEPS = 1
 WIDE = 256
+CROSS = ((0, 0), (7, 7), (6, 6), (5, 3), (4, 2), (3, 5), (2, 4), (1, 1))
 VMEM = pl.BlockSpec(memory_space=pltpu.VMEM)
 HBM = pl.BlockSpec(memory_space=pltpu.HBM)
 
@@ -422,12 +423,12 @@
                 out_ref[c, at : at + TILE, :] = piece[c * TILE : (c + 1) * TILE, :]
 
 
-def second_kernel(plan, scaling, *refs):
+def second_far_kernel(plan, scaling, *refs):
     slabs = refs[: plan.cols]
-    usual_ref, first_ref, out_ref, held_ref, rhs_ref = refs[plan.cols :]
-    row, col = lax.axis_index("row"), lax.axis_index("col")
-    for s in range(plan.cols):
-        held_ref[col ^ s] = slabs[s][...]
+    usual_ref, first_ref, out_ref, rhs_ref, held_ref = refs[plan.cols :]
+    col = lax.axis_index("col")
+    for s, pair in enumerate(crossing(plan.cols)):
+        held_ref[col ^ by_parity(col, sources(pair))] = slabs[s][...]
     sub, quarter = plan.sub, TILE // 2
     low = lax.broadcasted_iota(jnp.int32, (TILE, LANES), 0) < quarter
     for b9 in range(plan.half):
@@ -448,25 +449,40 @@
                     if n == plan.full:
                         value = turn_lanes(value, -inner * sub)
                     rhs_ref[i, at : at + TILE, n * LANES : (n + 1) * LANES] = value.astype(jnp.bfloat16)
+    other = 1 - lax.axis_index("row") // (plan.rows // 2)
+    transform(plan, scaling, other, usual_ref, first_ref, rhs_ref, out_ref)
+
+
+def second_near_kernel(plan, scaling, usual_ref, first_ref, rhs_ref, out_ref):
+    mine = lax.axis_index("row") // (plan.rows // 2)
+    transform(plan, scaling, mine, usual_ref, first_ref, rhs_ref, out_ref)
+
+
+def transform(plan, scaling, which, usual_ref, first_ref, rhs_ref, out_ref):
+    row = lax.axis_index("row")
+    sub = plan.sub
     wide = (plan.full + 1) * LANES
     lane = lane_index((1, wide))
     last = lane >= plan.full * LANES
     place = jnp.where(last, lane - plan.full * LANES + row * sub, lane & (LANES - 1))
     is_sine = place > GROUP // 2
     span = 2 * plan.block_b
-    total = plan.rows * span
+    devices = plan.rows // 2
+    size, total = devices * span, plan.rows * span
     tails = {}
     for i in range(plan.pairs):
         table = first_ref if i == 0 else usual_ref
-        both = dot(table[...], rhs_ref[i])
-        for r in range(plan.rows):
-            cosine, sine = both[r * span : (r + 1) * span, :], both[total + r * span : total + (r + 1) * span, :]
+        start = pl.multiple_of(which * size, TILE)
+        rows = jnp.concatenate([table[pl.ds(start, size), :], table[pl.ds(total + start, size), :]], axis=0)
+        both = dot(rows, rhs_ref[i])
+        for r in range(devices):
+            cosine, sine = both[r * span : (r + 1) * span, :], both[size + r * span : size + (r + 1) * span, :]
             merged = jnp.where(is_sine, sine, cosine) * scaling
             for f in range(plan.full):
                 at = f * plan.out_rows + i * span
                 out_ref[r, at : at + span, :] = merged[:, f * LANES : (f + 1) * LANES].astype(jnp.bfloat16)
             tails[i, r] = merged[:, plan.full * LANES :]
-    for r in range(plan.rows):
+    for r in range(devices):
         pieces = []
         for t in range(plan.row_tiles):
             i, at = divmod(t * TILE, span)
@@ -483,7 +499,7 @@
     return dot(ordered, unfold).astype(jnp.bfloat16)
 
 
-def early_kernel(plan, slab_ref, unfold_ref, order_ref, w_hbm, partial_ref, w_ref, own_ref, sems):
+def early_kernel(plan, slab_ref, unfold_ref, order_ref, w_hbm, partial_ref, w_ref, own_ref, raw_ref, sems):
     row = lax.axis_index("row")
     each = plan.full * GROUP
 
@@ -492,34 +508,38 @@
 
     copies = [pltpu.make_async_copy(part(0), own_ref, sems.at[0])]
     for s in range(1, plan.rows):
-        copies.append(pltpu.make_async_copy(part(s), w_ref.at[pl.ds((s - 1) * each, each), :], sems.at[s]))
+        copies.append(pltpu.make_async_copy(part(s), raw_ref.at[pl.ds((s - 1) * each, each), :], sems.at[s]))
     copies.append(
         pltpu.make_async_copy(
             w_hbm.at[pl.ds(plan.rows * each, GROUP), :],
-            w_ref.at[pl.ds((plan.rows - 1) * each, GROUP), :],
+            raw_ref.at[pl.ds((plan.rows - 1) * each, GROUP), :],
             sems.at[plan.rows],
         )
     )
     for copy in copies:
         copy.start()
-    spectrum = unfolded(plan, order_ref[...], unfold_ref[...], slab_ref)
+    unfold = unfold_ref[...]
+    spectrum = unfolded(plan, order_ref[...], unfold, slab_ref)
     copies[0].wait()
     for n in range(plan.features // WIDE):
         columns = slice(n * WIDE, (n + 1) * WIDE)
         partial_ref[:, columns] = dot(spectrum, own_ref[:, columns])
-    for copy in copies[1:]:
-        copy.wait()
+    for s in range(1, plan.rows + 1):
+        copies[s].wait()
+        size = each if s < plan.rows else GROUP
+        rows = slice((s - 1) * each, (s - 1) * each + size)
+        for n in range(plan.features // 512):
+            columns = slice(n * 512, (n + 1) * 512)
+            w_ref[rows, columns] = dot(unfold[:size, :size], raw_ref[rows, columns]).astype(jnp.bfloat16)
 
 
 def tail_kernel(plan, *refs):
     slabs = refs[: plan.rows]
-    unfold_ref, order_ref, partial_ref, w_ref, out_hbm, packed_ref, stage_ref, sems = refs[plan.rows :]
+    order_ref, partial_ref, w_ref, out_hbm, packed_ref, stage_ref, sems = refs[plan.rows :]
     row = lax.axis_index("row")
     main = plan.full * plan.out_rows
     for s in range(plan.rows):
         packed_ref[row ^ s] = slabs[s][main:, :]
-    order, unfold = order_ref[...], unfold_ref[...]
-    spectrum = [unfolded(plan, order, unfold, slabs[s]) for s in range(1, plan.rows)]
     packed = [packed_ref[q].astype(jnp.float32) for q in range(plan.rows)]
     turned = [[turn_lanes(value, plan.sub * t) for t in range(plan.rows)] for value in packed]
     pieces = []
@@ -529,15 +549,16 @@
         pieces.append(
             by_lane([turned[q][(q - inner) % plan.rows][rows, :] for q in range(plan.rows)], plan.sub)
         )
-    last = jnp.concatenate(pieces, axis=0).astype(jnp.bfloat16)
-    ordered = dot(order, last).astype(jnp.bfloat16)
-    spectrum.append(dot(ordered, unfold[:GROUP, :GROUP]).astype(jnp.bfloat16))
-    spectrum = jnp.concatenate(spectrum, axis=1)
+    parts = []
+    for s in range(1, plan.rows):
+        parts += [slabs[s][f * plan.out_rows : (f + 1) * plan.out_rows, :] for f in range(plan.full)]
+    parts.append(jnp.concatenate(pieces, axis=0).astype(jnp.bfloat16))
+    ordered = dot(order_ref[...], jnp.concatenate(parts, axis=1)).astype(jnp.bfloat16)
     group = 2 * plan.pairs
     copies = []
     for n in range(plan.features // WIDE):
         columns = slice(n * WIDE, (n + 1) * WIDE)
-        result = (partial_ref[:, columns] + dot(spectrum, w_ref[:, columns])).astype(jnp.bfloat16)
+        result = (partial_ref[:, columns] + dot(ordered, w_ref[:, columns])).astype(jnp.bfloat16)
         for k in range(plan.block_b):
             stage_ref[n, k] = result[k * group : (k + 1) * group, :]
         copy = pltpu.make_async_copy(stage_ref.at[n], out_hbm.at[:, :, pl.ds(n * WIDE, WIDE)], sems.at[n])
@@ -555,19 +576,34 @@
     return pltpu.CompilerParams(vmem_limit_bytes=mebibytes * 2**20)
 
 
-def exchange(values, axis, size):
+def by_parity(index, pair):
+    return pair[0] + (index % 2) * (pair[1] - pair[0])
+
+
+def sources(pair):
+    return pair if pair[0] % 2 == 0 else pair[::-1]
+
+
+def exchange(values, axis, size, pairs=None):
     here = lax.axis_index(axis)
     out = []
     for s in range(size):
+        pair = pairs[s] if pairs else (s, s)
+        there = here ^ by_parity(here, pair)
         if isinstance(values, tuple):
-            source, index = values[2 * s // size], (here ^ s) % (size // 2)
+            source, index = values[2 * s // size], there % (size // 2)
         else:
-            source, index = values, here ^ s
+            source, index = values, there
         slab = lax.dynamic_index_in_dim(source, index, 0, keepdims=False)
         if s:
-            slab = lax.ppermute(slab, axis, [(n, n ^ s) for n in range(size)])
+            slab = lax.ppermute(slab, axis, [(n, n ^ pair[n % 2]) for n in range(size)])
         out.append(slab)
     return out
+
+
+def crossing(cols):
+    pairs = [(s, s) for s in range(cols)]
+    return CROSS if cols == len(CROSS) else pairs
 
 
 def packed(plan, tokens, norm_gain, w_in, w_out):
@@ -629,25 +665,33 @@
         cost_estimate=estimate(10**8, 10**6),
         name="first",
     )(*slabs, first)
-    slabs = exchange(turned, "col", plan.cols)
+    slabs = exchange(turned, "col", plan.cols, crossing(plan.cols))
     usual, special = (jnp.asarray(table, half_type) for table in second_tables(plan))
     usual, special = (table.reshape(-1, table.shape[-1]) for table in (usual, special))
     leading = jnp.where(col == 0, special, usual)
     depth = plan.half * plan.cols * 4
-    back = pl.pallas_call(
-        functools.partial(second_kernel, plan, scaling),
-        out_shape=jax.ShapeDtypeStruct((plan.rows, plan.back_rows, LANES), half_type),
+    slab = pltpu.VMEM((plan.rows // 2, plan.back_rows, LANES), half_type)
+    rhs = pltpu.VMEM((plan.pairs, depth, (plan.full + 1) * LANES), half_type)
+    back_far, rhs = pl.pallas_call(
+        functools.partial(second_far_kernel, plan, scaling),
+        out_shape=(slab, rhs),
         in_specs=[VMEM] * (plan.cols + 2),
-        out_specs=VMEM,
-        scratch_shapes=[
-            pltpu.VMEM((plan.cols, plan.tiles * TILE, LANES), half_type),
-            pltpu.VMEM((plan.pairs, depth, (plan.full + 1) * LANES), half_type),
-        ],
+        out_specs=(VMEM, VMEM),
+        scratch_shapes=[pltpu.VMEM((plan.cols, plan.tiles * TILE, LANES), half_type)],
         compiler_params=limit(12),
         cost_estimate=estimate(3 * 10**8, 10**6),
-        name="second",
+        name="second_far",
     )(*slabs, usual, leading)
-    slabs = exchange(back, "row", plan.rows)
+    back_near = pl.pallas_call(
+        functools.partial(second_near_kernel, plan, scaling),
+        out_shape=slab,
+        in_specs=[VMEM] * 3,
+        out_specs=VMEM,
+        compiler_params=limit(12),
+        cost_estimate=estimate(3 * 10**8, 10**6),
+        name="second_near",
+    )(usual, leading, rhs)
+    slabs = exchange((back_near, back_far), "row", plan.rows)
     unfold = jnp.asarray(paired(unfold_table()), half_type)
     order = jnp.asarray(order_table(plan), half_type)
     main, each = plan.full * plan.out_rows, plan.full * GROUP
@@ -660,15 +704,19 @@
         ),
         in_specs=[VMEM] * 3 + [HBM],
         out_specs=(VMEM, VMEM),
-        scratch_shapes=[pltpu.VMEM((each, features), half_type), pltpu.SemaphoreType.DMA((plan.rows + 1,))],
-        compiler_params=limit(8),
+        scratch_shapes=[
+            pltpu.VMEM((each, features), half_type),
+            pltpu.VMEM((channels - each, features), half_type),
+            pltpu.SemaphoreType.DMA((plan.rows + 1,)),
+        ],
+        compiler_params=limit(14),
         cost_estimate=cost,
         name="early",
     )(slabs[0], unfold, order, pltpu.with_memory_space_constraint(w_out, pltpu.HBM))
     return pl.pallas_call(
         functools.partial(tail_kernel, plan),
         out_shape=jax.ShapeDtypeStruct((plan.block_b, 2 * plan.pairs, features), half_type),
-        in_specs=[VMEM] * (plan.rows + 4),
+        in_specs=[VMEM] * (plan.rows + 3),
         out_specs=HBM,
         scratch_shapes=[
             pltpu.VMEM((plan.rows, plan.back_rows - main, LANES), half_type),
@@ -678,7 +726,7 @@
         compiler_params=limit(12),
         cost_estimate=cost,
         name="tail",
-    )(*slabs, unfold, order, partial, w_rest)
+    )(*slabs, order, partial, w_rest)
 
 
 def shards(tokens, norm_gain, w_in, w_out):

time: 41.7 us -> 44.3 us (1.062)
  waiting for transfers between devices: 13 us -> 15.5 us
  Pallas kernels: 10.6 us -> 11.6 us
  starting transfers between devices: 16.6 us -> 15.8 us
    ppermute x13, waiting for transfers between devices: 13 us -> 15.5 us  [exchange(): slab = lax.ppermute(slab, axis, [(n, n ^ pair[n % 2]) for n in range(size)])]
    pallas_call x1, Pallas kernels: 2.37 us -> 3.24 us  [packed(): pl.pallas_call(functools.partial(early_kernel, plan), out_shape=(pltpu.VM...]
    ppermute x13, starting transfers between devices: 16.6 us -> 15.8 us  [exchange(): slab = lax.ppermute(slab, axis, [(n, n ^ pair[n % 2]) for n in range(size)])]
    pallas_call x1 -> x2, Pallas kernels: 0.87 us -> 1.11 us  [the longest x1 0.61 us: packed(): pl.pallas_call(functools.partial(second_far_kernel, plan, scaling), out_s...]
  transfers between devices with their start and end apart: 13 -> 13, of which waited for: 7 -> 7; matrix products, arithmetic and copies ran while one was open for 2% -> 2% of each run, Pallas kernels for 6% -> 7%
where the time goes in v2:
time: 44.3 us; the launch traced here: 44.1 us
  starting transfers between devices  15.8 us (36%)
  waiting for transfers between devices  15.5 us (35%)
  Pallas kernels  11.6 us (26%)
  local copies, waits for them, and re-layouts  1.07 us (2%)
    ppermute x13, starting transfers between devices, exchange(): slab = lax.ppermute(slab, axis, [(n, n ^ pair[n % 2]) for n in range(size)])  15.8 us
    ppermute x13, waiting for transfers between devices, exchange(): slab = lax.ppermute(slab, axis, [(n, n ^ pair[n % 2]) for n in range(size)])  15.5 us
    pallas_call x1, Pallas kernels, packed(): pl.pallas_call(functools.partial(early_kernel, plan), out_shape=(pltpu.VM...  3.24 us
    pallas_call x1, Pallas kernels, packed(): pl.pallas_call(functools.partial(far_kernel, plan, depth), out_shape=(plt...  2.88 us
    pallas_call x1, Pallas kernels, packed(): pl.pallas_call(functools.partial(near_kernel, plan, depth), out_shape=plt...  2.43 us
    pallas_call x1, Pallas kernels, packed(): pl.pallas_call(functools.partial(tail_kernel, plan), out_shape=jax.ShapeD...  1.65 us
    squeeze x1, local copies, waits for them, and re-layouts, packed(): lax.dynamic_index_in_dim(jnp.asarray(first_tables(plan), half_type), col,...  0.92 us
  transfers between devices with their start and end apart: 13, of which 7 were waited for; matrix products, arithmetic and copies ran while one was open for 2% of the time, Pallas kernels for 7%

profile of v2, /device:TPU:0, one launch (start us, length us, event | category | flops | bytes accessed | tf_op | source)
XLA Modules:
  0.0 44.1 jit_solution(17145556825980806989)
XLA Ops:
  0.0 2.9 %far.1 = (bf16[2,336,128]{2,1,0:T(8,128)(2,1)S(1)}, bf16[2,48,128]{2,1,0:T(8,128)(2,1)S(1)}, bf16[144,2048]{1,0:T(8,128)(2,1)S(1)}) custom-call(bf16[144,2048]{1,0:T(8,128)(2,1)} %bitcast.38, bf16[16,128]{1,0:T(8,128)(2,1)} %bitcast.39, bf16[2048,1152]{1,0:T(8,128)(2,1)} %w_hbm.4, bf16[256,256]{1,0:T(8,128)(2,1)} %constant.120.clone.table_hbm), custom_call_target="tpu_custom_call" | custom-call | flops 339738624 | bytes 2359296 | tf_op jit(solution)/shard_map/far/pallas_call | solution.py:620
  2.9 0.0 copy-start
  2.9 0.0 copy-start.3
  2.9 2.4 %near.1 = bf16[2,336,128]{2,1,0:T(8,128)(2,1)S(1)} custom-call(bf16[144,2048]{1,0:T(8,128)(2,1)S(1)} %get-tuple-element.12.normed_ref, bf16[2,48,128]{2,1,0:T(8,128)(2,1)S(1)} %get-tuple-element.13.near_ref, bf16[2048,1152]{1,0:T(8,128)(2,1)} %w_hbm.4, bf16[256,256]{1,0:T(8,128)(2,1)} %constant.120.clone.table_hbm), custom_call_target="tpu_custom_call" | custom-call | flops 339738624 | bytes 2359296 | tf_op jit(solution)/shard_map/near/pallas_call | solution.py:641
  5.3 0.0 copy-start.1
  5.4 3.1 %collective-permute-start = (bf16[336,128]{1,0:T(8,128)(2,1)S(1)}, bf16[336,128]{1,0:T(8,128)(2,1)S(1)}, u32[]{:S(2)}, u32[]{:S(2)}) collective-permute-start(bf16[336,128]{1,0:T(8,128)(2,1)S(1)} %get-tuple-element.29), channel_id=1, source_target_pairs={{0,8},{8,0},{16,24},{24,16},{1,9},{9,1},{17,25},{25,17},{2,10},{10... | collective-permute-start | bytes 258056 | tf_op jit(solution)/shard_map/ppermute | solution.py:599
  8.5 2.5 %collective-permute-start.2 = (bf16[336,128]{1,0:T(8,128)(2,1)S(1)}, bf16[336,128]{1,0:T(8,128)(2,1)S(1)}, u32[]{:S(2)}, u32[]{:S(2)}) collective-permute-start(bf16[336,128]{1,0:T(8,128)(2,1)S(1)} %get-tuple-element.27), channel_id=1, source_target_pairs={{0,24},{8,16},{16,8},{24,0},{1,25},{9,17},{17,9},{25,1},{2,26},{10... | collective-permute-start | bytes 258056 | tf_op jit(solution)/shard_map/ppermute | solution.py:599
  11.1 0.2 collective-permute-start.1
  11.3 0.9 %dynamic-slice_bitcast_fusion.refs_4_ = bf16[9,64,64]{2,1,0:T(8,128)(2,1)S(1)} fusion(bf16[8,9,64,64]{3,2,1,0:T(8,128)(2,1)} %constant.121.clone, s32[]{:T(128)S(6)} %select_n.100), kind=kLoop, calls=%fused_computation.1 | loop fusion | bytes 147460 | tf_op jit(solution)/shard_map/jit(dynamic_index_in_dim)/squeeze | solution.py:657
  12.2 4.1 %collective-permute-done.2.refs_3_ = bf16[336,128]{1,0:T(8,128)(2,1)S(1)} collective-permute-done((bf16[336,128]{1,0:T(8,128)(2,1)S(1)}, bf16[336,128]{1,0:T(8,128)(2,1)S(1)}, u32[]{:S(2)}, u32[]{:S(2)}) %collective-permute-start.2) | collective-permute-done | bytes 86048 | tf_op jit(solution)/shard_map/ppermute | solution.py:599
  16.3 2.8 %collective-permute-done.1.refs_2_ = bf16[336,128]{1,0:T(8,128)(2,1)S(1)} collective-permute-done((bf16[336,128]{1,0:T(8,128)(2,1)S(1)}, bf16[336,128]{1,0:T(8,128)(2,1)S(1)}, u32[]{:S(2)}, u32[]{:S(2)}) %collective-permute-start.1) | collective-permute-done | bytes 86048 | tf_op jit(solution)/shard_map/ppermute | solution.py:599
  19.1 0.3 first.1
  19.5 0.1 collective-permute-start.9
  19.5 1.6 %collective-permute-start.8 = (bf16[168,128]{1,0:T(8,128)(2,1)S(1)}, bf16[168,128]{1,0:T(8,128)(2,1)S(1)}, u32[]{:S(2)}, u32[]{:S(2)}) collective-permute-start(bf16[168,128]{1,0:T(8,128)(2,1)S(1)} %get-tuple-element.20), channel_id=1, source_target_pairs={{0,2},{1,5},{2,0},{3,7},{4,6},{5,1},{6,4},{7,3},{8,10},{9,13},{10,... | collective-permute-start | bytes 129032 | tf_op jit(solution)/shard_map/ppermute | solution.py:599
  21.1 1.3 %collective-permute-start.7 = (bf16[168,128]{1,0:T(8,128)(2,1)S(1)}, bf16[168,128]{1,0:T(8,128)(2,1)S(1)}, u32[]{:S(2)}, u32[]{:S(2)}) collective-permute-start(bf16[168,128]{1,0:T(8,128)(2,1)S(1)} %get-tuple-element.21), channel_id=1, source_target_pairs={{0,3},{1,4},{2,1},{3,6},{4,7},{5,0},{6,5},{7,2},{8,11},{9,12},{10,... | collective-permute-start | bytes 129032 | tf_op jit(solution)/shard_map/ppermute | solution.py:599
  22.4 0.5 %collective-permute-start.6 = (bf16[168,128]{1,0:T(8,128)(2,1)S(1)}, bf16[168,128]{1,0:T(8,128)(2,1)S(1)}, u32[]{:S(2)}, u32[]{:S(2)}) collective-permute-start(bf16[168,128]{1,0:T(8,128)(2,1)S(1)} %get-tuple-element.22), channel_id=1, source_target_pairs={{0,4},{1,3},{2,6},{3,1},{4,0},{5,7},{6,2},{7,5},{8,12},{9,11},{10,... | collective-permute-start | bytes 129032 | tf_op jit(solution)/shard_map/ppermute | solution.py:599
  22.9 0.2 collective-permute-start.5
  23.1 2.4 %collective-permute-start.4 = (bf16[168,128]{1,0:T(8,128)(2,1)S(1)}, bf16[168,128]{1,0:T(8,128)(2,1)S(1)}, u32[]{:S(2)}, u32[]{:S(2)}) collective-permute-start(bf16[168,128]{1,0:T(8,128)(2,1)S(1)} %get-tuple-element.24), channel_id=1, source_target_pairs={{0,6},{1,7},{2,4},{3,5},{4,2},{5,3},{6,0},{7,1},{8,14},{9,15},{10,... | collective-permute-start | bytes 129032 | tf_op jit(solution)/shard_map/ppermute | solution.py:599
  25.6 0.2 collective-permute-start.3
  25.8 0.1 broadcast_select_fusion.refs_9_.first_ref
  25.9 0.5 %collective-permute-done.6.refs_4_ = bf16[168,128]{1,0:T(8,128)(2,1)S(1)} collective-permute-done((bf16[168,128]{1,0:T(8,128)(2,1)S(1)}, bf16[168,128]{1,0:T(8,128)(2,1)S(1)}, u32[]{:S(2)}, u32[]{:S(2)}) %collective-permute-start.6) | collective-permute-done | bytes 43040 | tf_op jit(solution)/shard_map/ppermute | solution.py:599
  26.4 1.8 %collective-permute-done.4.refs_2_ = bf16[168,128]{1,0:T(8,128)(2,1)S(1)} collective-permute-done((bf16[168,128]{1,0:T(8,128)(2,1)S(1)}, bf16[168,128]{1,0:T(8,128)(2,1)S(1)}, u32[]{:S(2)}, u32[]{:S(2)}) %collective-permute-start.4) | collective-permute-done | bytes 43040 | tf_op jit(solution)/shard_map/ppermute | solution.py:599
  28.2 1.8 %collective-permute-done.3.refs_1_ = bf16[168,128]{1,0:T(8,128)(2,1)S(1)} collective-permute-done((bf16[168,128]{1,0:T(8,128)(2,1)S(1)}, bf16[168,128]{1,0:T(8,128)(2,1)S(1)}, u32[]{:S(2)}, u32[]{:S(2)}) %collective-permute-start.3) | collective-permute-done | bytes 43040 | tf_op jit(solution)/shard_map/ppermute | solution.py:599
  30.0 0.6 %second_far.1 = (bf16[2,328,128]{2,1,0:T(8,128)(2,1)S(1)}, bf16[2,288,384]{2,1,0:T(8,128)(2,1)S(1)}) custom-call(bf16[168,128]{1,0:T(8,128)(2,1)S(1)} %get-tuple-element.26.refs_0_, bf16[168,128]{1,0:T(8,128)(2,1)S(1)} %collective-permute-done.3.refs_1_, bf16[168,128]{1,0:T(8,128)(2,1)S(1)} %collective-permute-done.4.refs_2_, ...), custom_call_target="tpu_custom_call" | custom-call | flops 300000000 | bytes 1000000 | tf_op jit(solution)/shard_map/second_far/pallas_call | solution.py:675
  30.6 0.5 %second_near.1 = bf16[2,328,128]{2,1,0:T(8,128)(2,1)S(1)} custom-call(bf16[576,288]{1,0:T(8,128)(2,1)S(1)} %copy-done, bf16[576,288]{1,0:T(8,128)(2,1)S(1)} %broadcast_select_fusion.refs_9_.first_ref, bf16[2,288,384]{2,1,0:T(8,128)(2,1)S(1)} %get-tuple-element.15.rhs_ref), custom_call_target="tpu_custom_call" | custom-call | flops 300000000 | bytes 1000000 | tf_op jit(solution)/shard_map/second_near/pallas_call | solution.py:685
  31.2 0.1 collective-permute-start.10
  31.3 2.6 %collective-permute-start.12 = (bf16[328,128]{1,0:T(8,128)(2,1)S(1)}, bf16[328,128]{1,0:T(8,128)(2,1)S(1)}, u32[]{:S(2)}, u32[]{:S(2)}) collective-permute-start(bf16[328,128]{1,0:T(8,128)(2,1)S(1)} %get-tuple-element.31), channel_id=1, source_target_pairs={{0,24},{8,16},{16,8},{24,0},{1,25},{9,17},{17,9},{25,1},{2,26},{10... | collective-permute-start | bytes 251912 | tf_op jit(solution)/shard_map/ppermute | solution.py:599
  33.9 1.0 %collective-permute-start.11 = (bf16[328,128]{1,0:T(8,128)(2,1)S(1)}, bf16[328,128]{1,0:T(8,128)(2,1)S(1)}, u32[]{:S(2)}, u32[]{:S(2)}) collective-permute-start(bf16[328,128]{1,0:T(8,128)(2,1)S(1)} %get-tuple-element.32), channel_id=1, source_target_pairs={{0,16},{8,24},{16,0},{24,8},{1,17},{9,25},{17,1},{25,9},{2,18},{10... | collective-permute-start | bytes 251912 | tf_op jit(solution)/shard_map/ppermute | solution.py:599
  34.8 3.2 %early.1 = (f32[144,2048]{1,0:T(8,128)S(1)}, bf16[896,2048]{1,0:T(8,128)(2,1)S(1)}) custom-call(bf16[328,128]{1,0:T(8,128)(2,1)S(1)} %get-tuple-element.34.slab_ref.refs_0_, bf16[256,256]{1,0:T(8,128)(2,1)S(1)} %copy-done.2, bf16[144,144]{1,0:T(8,128)(2,1)S(1)} %copy-done.1, bf16[1152,2048]{1,0:T(8,128)(2,1)} %w_hbm.5), custom_call_target="tpu_custom_call" | custom-call | flops 339738624 | bytes 2359296 | tf_op jit(solution)/shard_map/early/pallas_call | solution.py:699
  38.1 0.9 %collective-permute-done.12.refs_3_ = bf16[328,128]{1,0:T(8,128)(2,1)S(1)} collective-permute-done((bf16[328,128]{1,0:T(8,128)(2,1)S(1)}, bf16[328,128]{1,0:T(8,128)(2,1)S(1)}, u32[]{:S(2)}, u32[]{:S(2)}) %collective-permute-start.12) | collective-permute-done | bytes 84000 | tf_op jit(solution)/shard_map/ppermute | solution.py:599
  39.0 3.5 %collective-permute-done.11.refs_2_ = bf16[328,128]{1,0:T(8,128)(2,1)S(1)} collective-permute-done((bf16[328,128]{1,0:T(8,128)(2,1)S(1)}, bf16[328,128]{1,0:T(8,128)(2,1)S(1)}, u32[]{:S(2)}, u32[]{:S(2)}) %collective-permute-start.11) | collective-permute-done | bytes 84000 | tf_op jit(solution)/shard_map/ppermute | solution.py:599
  42.5 1.6 %tail.1 = bf16[36,4,2048]{2,1,0:T(4,128)(2,1)} custom-call(bf16[328,128]{1,0:T(8,128)(2,1)S(1)} %get-tuple-element.34.slab_ref.refs_0_, bf16[328,128]{1,0:T(8,128)(2,1)S(1)} %collective-permute-done.10.refs_1_, bf16[328,128]{1,0:T(8,128)(2,1)S(1)} %collective-permute-done.11.refs_2_, bf16[328,128]{1,0:T(8,128)(2,1)S(1)} %collective-permute-done.12.refs_3_, ...), custom_call_target="tpu_custom_call" | custom-call | flops 339738624 | bytes 2359296 | tf_op jit(solution)/shard_map/tail/pallas_call | solution.py:716
  (16 shorter events, 0.2 us)
Async XLA Ops:
  2.9 22.9 %copy-start = (bf16[576,288]{1,0:T(8,128)(2,1)S(1)}, bf16[576,288]{1,0:T(8,128)(2,1)}, u32[]{:S(2)}) copy-start(bf16[576,288]{1,0:T(8,128)(2,1)} %constant.127.refs_8_.usual_ref) | copy-start | bytes 995332
  2.9 22.9 %copy-start.3 = (bf16[576,288]{1,0:T(8,128)(2,1)S(1)}, bf16[576,288]{1,0:T(8,128)(2,1)}, u32[]{:S(2)}) copy-start(bf16[576,288]{1,0:T(8,128)(2,1)} %constant.128) | copy-start | bytes 995332
  5.3 29.5 %copy-start.1 = (bf16[144,144]{1,0:T(8,128)(2,1)S(1)}, bf16[144,144]{1,0:T(8,128)(2,1)}, u32[]{:S(2)}) copy-start(bf16[144,144]{1,0:T(8,128)(2,1)} %constant.125.clone.order_ref.refs_4_) | copy-start | bytes 124420
  5.4 29.5 %copy-start.2 = (bf16[256,256]{1,0:T(8,128)(2,1)S(1)}, bf16[256,256]{1,0:T(8,128)(2,1)}, u32[]{:S(2)}) copy-start(bf16[256,256]{1,0:T(8,128)(2,1)} %constant.124.clone.unfold_ref) | copy-start | bytes 393220
  5.4 6.8 %collective-permute-start = (bf16[336,128]{1,0:T(8,128)(2,1)S(1)}, bf16[336,128]{1,0:T(8,128)(2,1)S(1)}, u32[]{:S(2)}, u32[]{:S(2)}) collective-permute-start(bf16[336,128]{1,0:T(8,128)(2,1)S(1)} %get-tuple-element.29), channel_id=1, source_target_pairs={{0,8},{8,0},{16,24},{24,16},{1,9},{9,1},{17,25},{25,17},{2,10},{10... | collective-permute-start | bytes 258056 | tf_op jit(solution)/shard_map/ppermute | solution.py:599
  8.5 7.8 %collective-permute-start.2 = (bf16[336,128]{1,0:T(8,128)(2,1)S(1)}, bf16[336,128]{1,0:T(8,128)(2,1)S(1)}, u32[]{:S(2)}, u32[]{:S(2)}) collective-permute-start(bf16[336,128]{1,0:T(8,128)(2,1)S(1)} %get-tuple-element.27), channel_id=1, source_target_pairs={{0,24},{8,16},{16,8},{24,0},{1,25},{9,17},{17,9},{25,1},{2,26},{10... | collective-permute-start | bytes 258056 | tf_op jit(solution)/shard_map/ppermute | solution.py:599
  11.1 8.0 %collective-permute-start.1 = (bf16[336,128]{1,0:T(8,128)(2,1)S(1)}, bf16[336,128]{1,0:T(8,128)(2,1)S(1)}, u32[]{:S(2)}, u32[]{:S(2)}) collective-permute-start(bf16[336,128]{1,0:T(8,128)(2,1)S(1)} %get-tuple-element.28), channel_id=1, source_target_pairs={{0,16},{8,24},{16,0},{24,8},{1,17},{9,25},{17,1},{25,9},{2,18},{10... | collective-permute-start | bytes 258056 | tf_op jit(solution)/shard_map/ppermute | solution.py:599
  19.5 3.6 %collective-permute-start.9 = (bf16[168,128]{1,0:T(8,128)(2,1)S(1)}, bf16[168,128]{1,0:T(8,128)(2,1)S(1)}, u32[]{:S(2)}, u32[]{:S(2)}) collective-permute-start(bf16[168,128]{1,0:T(8,128)(2,1)S(1)} %get-tuple-element.19), channel_id=1, source_target_pairs={{0,1},{1,0},{2,3},{3,2},{4,5},{5,4},{6,7},{7,6},{8,9},{9,8},{10,11... | collective-permute-start | bytes 129032 | tf_op jit(solution)/shard_map/ppermute | solution.py:599
  19.5 6.0 %collective-permute-start.8 = (bf16[168,128]{1,0:T(8,128)(2,1)S(1)}, bf16[168,128]{1,0:T(8,128)(2,1)S(1)}, u32[]{:S(2)}, u32[]{:S(2)}) collective-permute-start(bf16[168,128]{1,0:T(8,128)(2,1)S(1)} %get-tuple-element.20), channel_id=1, source_target_pairs={{0,2},{1,5},{2,0},{3,7},{4,6},{5,1},{6,4},{7,3},{8,10},{9,13},{10,... | collective-permute-start | bytes 129032 | tf_op jit(solution)/shard_map/ppermute | solution.py:599
  21.1 4.8 %collective-permute-start.7 = (bf16[168,128]{1,0:T(8,128)(2,1)S(1)}, bf16[168,128]{1,0:T(8,128)(2,1)S(1)}, u32[]{:S(2)}, u32[]{:S(2)}) collective-permute-start(bf16[168,128]{1,0:T(8,128)(2,1)S(1)} %get-tuple-element.21), channel_id=1, source_target_pairs={{0,3},{1,4},{2,1},{3,6},{4,7},{5,0},{6,5},{7,2},{8,11},{9,12},{10,... | collective-permute-start | bytes 129032 | tf_op jit(solution)/shard_map/ppermute | solution.py:599
  22.4 4.0 %collective-permute-start.6 = (bf16[168,128]{1,0:T(8,128)(2,1)S(1)}, bf16[168,128]{1,0:T(8,128)(2,1)S(1)}, u32[]{:S(2)}, u32[]{:S(2)}) collective-permute-start(bf16[168,128]{1,0:T(8,128)(2,1)S(1)} %get-tuple-element.22), channel_id=1, source_target_pairs={{0,4},{1,3},{2,6},{3,1},{4,0},{5,7},{6,2},{7,5},{8,12},{9,11},{10,... | collective-permute-start | bytes 129032 | tf_op jit(solution)/shard_map/ppermute | solution.py:599
  22.9 3.5 %collective-permute-start.5 = (bf16[168,128]{1,0:T(8,128)(2,1)S(1)}, bf16[168,128]{1,0:T(8,128)(2,1)S(1)}, u32[]{:S(2)}, u32[]{:S(2)}) collective-permute-start(bf16[168,128]{1,0:T(8,128)(2,1)S(1)} %get-tuple-element.23), channel_id=1, source_target_pairs={{0,5},{1,2},{2,7},{3,0},{4,1},{5,6},{6,3},{7,4},{8,13},{9,10},{10,... | collective-permute-start | bytes 129032 | tf_op jit(solution)/shard_map/ppermute | solution.py:599
  23.1 5.1 %collective-permute-start.4 = (bf16[168,128]{1,0:T(8,128)(2,1)S(1)}, bf16[168,128]{1,0:T(8,128)(2,1)S(1)}, u32[]{:S(2)}, u32[]{:S(2)}) collective-permute-start(bf16[168,128]{1,0:T(8,128)(2,1)S(1)} %get-tuple-element.24), channel_id=1, source_target_pairs={{0,6},{1,7},{2,4},{3,5},{4,2},{5,3},{6,0},{7,1},{8,14},{9,15},{10,... | collective-permute-start | bytes 129032 | tf_op jit(solution)/shard_map/ppermute | solution.py:599
  25.6 4.5 %collective-permute-start.3 = (bf16[168,128]{1,0:T(8,128)(2,1)S(1)}, bf16[168,128]{1,0:T(8,128)(2,1)S(1)}, u32[]{:S(2)}, u32[]{:S(2)}) collective-permute-start(bf16[168,128]{1,0:T(8,128)(2,1)S(1)} %get-tuple-element.25), channel_id=1, source_target_pairs={{0,7},{1,6},{2,5},{3,4},{4,3},{5,2},{6,1},{7,0},{8,15},{9,14},{10,... | collective-permute-start | bytes 129032 | tf_op jit(solution)/shard_map/ppermute | solution.py:599
  31.2 6.9 %collective-permute-start.10 = (bf16[328,128]{1,0:T(8,128)(2,1)S(1)}, bf16[328,128]{1,0:T(8,128)(2,1)S(1)}, u32[]{:S(2)}, u32[]{:S(2)}) collective-permute-start(bf16[328,128]{1,0:T(8,128)(2,1)S(1)} %get-tuple-element.33), channel_id=1, source_target_pairs={{0,8},{8,0},{16,24},{24,16},{1,9},{9,1},{17,25},{25,17},{2,10},{10... | collective-permute-start | bytes 251912 | tf_op jit(solution)/shard_map/ppermute | solution.py:599
  31.3 7.7 %collective-permute-start.12 = (bf16[328,128]{1,0:T(8,128)(2,1)S(1)}, bf16[328,128]{1,0:T(8,128)(2,1)S(1)}, u32[]{:S(2)}, u32[]{:S(2)}) collective-permute-start(bf16[328,128]{1,0:T(8,128)(2,1)S(1)} %get-tuple-element.31), channel_id=1, source_target_pairs={{0,24},{8,16},{16,8},{24,0},{1,25},{9,17},{17,9},{25,1},{2,26},{10... | collective-permute-start | bytes 251912 | tf_op jit(solution)/shard_map/ppermute | solution.py:599
  33.9 8.6 %collective-permute-start.11 = (bf16[328,128]{1,0:T(8,128)(2,1)S(1)}, bf16[328,128]{1,0:T(8,128)(2,1)S(1)}, u32[]{:S(2)}, u32[]{:S(2)}) collective-permute-start(bf16[328,128]{1,0:T(8,128)(2,1)S(1)} %get-tuple-element.32), channel_id=1, source_target_pairs={{0,16},{8,24},{16,0},{24,8},{1,17},{9,25},{17,1},{25,9},{2,18},{10... | collective-permute-start | bytes 251912 | tf_op jit(solution)/shard_map/ppermute | solution.py:599

commit v3 on v2

--- a/solution.py
+++ b/solution.py
@@ -126,7 +126,7 @@
 TILE = 8
 STEPS = 1
 WIDE = 256
-CROSS = ((0, 0), (7, 7), (6, 6), (5, 3), (4, 2), (3, 5), (2, 4), (1, 1))
+RELAYED = ((0, 0), (1, 1), (2, 4), (5, 3), (4, 2), (3, 5), (6, 6), (7, 7))
 VMEM = pl.BlockSpec(memory_space=pltpu.VMEM)
 HBM = pl.BlockSpec(memory_space=pltpu.HBM)
 
@@ -428,7 +428,7 @@
     usual_ref, first_ref, out_ref, rhs_ref, held_ref = refs[plan.cols :]
     col = lax.axis_index("col")
     for s, pair in enumerate(crossing(plan.cols)):
-        held_ref[col ^ by_parity(col, sources(pair))] = slabs[s][...]
+        held_ref[col ^ by_parity(col, pair)] = slabs[s][: plan.tiles * TILE, :]
     sub, quarter = plan.sub, TILE // 2
     low = lax.broadcasted_iota(jnp.int32, (TILE, LANES), 0) < quarter
     for b9 in range(plan.half):
@@ -580,30 +580,51 @@
     return pair[0] + (index % 2) * (pair[1] - pair[0])
 
 
-def sources(pair):
-    return pair if pair[0] % 2 == 0 else pair[::-1]
-
-
-def exchange(values, axis, size, pairs=None):
+def exchange(values, axis, size):
     here = lax.axis_index(axis)
     out = []
     for s in range(size):
-        pair = pairs[s] if pairs else (s, s)
-        there = here ^ by_parity(here, pair)
+        there = here ^ s
         if isinstance(values, tuple):
             source, index = values[2 * s // size], there % (size // 2)
         else:
             source, index = values, there
         slab = lax.dynamic_index_in_dim(source, index, 0, keepdims=False)
         if s:
-            slab = lax.ppermute(slab, axis, [(n, n ^ pair[n % 2]) for n in range(size)])
+            slab = lax.ppermute(slab, axis, [(n, n ^ s) for n in range(size)])
         out.append(slab)
     return out
 
 
 def crossing(cols):
-    pairs = [(s, s) for s in range(cols)]
-    return CROSS if cols == len(CROSS) else pairs
+    if cols == len(RELAYED):
+        return RELAYED
+    return tuple((s, s) for s in range(cols))
+
+
+def cross(values, cols):
+    if cols != len(RELAYED):
+        return exchange(values, "col", cols)
+    here = lax.axis_index("col")
+
+    def slab(pair, flip=0):
+        return lax.dynamic_index_in_dim(values, here ^ by_parity(here, pair) ^ flip, 0, keepdims=False)
+
+    def send(value, pair):
+        return lax.ppermute(value, "col", [(n, n ^ pair[n % 2]) for n in range(cols)])
+
+    def both(pair):
+        return jnp.concatenate([slab(pair), slab(pair, 1)], axis=0)
+
+    rows = values.shape[1]
+    diagonal = send(both((6, 6)), (6, 6))
+    beside = send(both((4, 2)), (4, 2))
+    crossed = send(slab((3, 5)), (3, 5))
+    straight = send(slab((2, 4)), (2, 4))
+    sibling = send(slab((1, 1)), (1, 1))
+    diagonal_other = send(diagonal[rows:], (1, 1))
+    beside_other = send(beside[rows:], (1, 1))
+    return [slab((0, 0)), sibling, straight, crossed, beside, beside_other, diagonal, diagonal_other]
 
 
 def packed(plan, tokens, norm_gain, w_in, w_out):
@@ -665,7 +686,7 @@
         cost_estimate=estimate(10**8, 10**6),
         name="first",
     )(*slabs, first)
-    slabs = exchange(turned, "col", plan.cols, crossing(plan.cols))
+    slabs = cross(turned, plan.cols)
     usual, special = (jnp.asarray(table, half_type) for table in second_tables(plan))
     usual, special = (table.reshape(-1, table.shape[-1]) for table in (usual, special))
     leading = jnp.where(col == 0, special, usual)

time: 44.3 us -> 42.1 us (0.950)
  starting transfers between devices: 15.8 us -> 14.4 us
  waiting for transfers between devices: 15.5 us -> 14.5 us
    ppermute x13, starting transfers between devices: 15.8 us -> 14.4 us  [the longest x6 9.46 us: exchange(): slab = lax.ppermute(slab, axis, [(n, n ^ s) for n in range(size)])]
    ppermute x13, waiting for transfers between devices: 15.5 us -> 14.5 us  [the longest x6 11.3 us: exchange(): slab = lax.ppermute(slab, axis, [(n, n ^ s) for n in range(size)])]
  transfers between devices with their start and end apart: 13 -> 13, of which waited for: 7 -> 7; matrix products, arithmetic and copies ran while one was open for 2% -> 2% of each run, Pallas kernels for 7% -> 8%
where the time goes in v3:
time: 42.1 us; the launch traced here: 41.9 us
  waiting for transfers between devices  14.5 us (34%)
  starting transfers between devices  14.4 us (34%)
  Pallas kernels  11.6 us (28%)
  local copies, waits for them, and re-layouts  1.08 us (3%)
    ppermute x6, waiting for transfers between devices, exchange(): slab = lax.ppermute(slab, axis, [(n, n ^ s) for n in range(size)])  11.3 us
    ppermute x6, starting transfers between devices, exchange(): slab = lax.ppermute(slab, axis, [(n, n ^ s) for n in range(size)])  9.46 us
    ppermute x7, starting transfers between devices, send(): lax.ppermute(value, 'col', [(n, n ^ pair[n % 2]) for n in range(cols)])  4.95 us
    pallas_call x1, Pallas kernels, packed(): pl.pallas_call(functools.partial(early_kernel, plan), out_shape=(pltpu.VM...  3.25 us
    ppermute x7, waiting for transfers between devices, send(): lax.ppermute(value, 'col', [(n, n ^ pair[n % 2]) for n in range(cols)])  3.24 us
    pallas_call x1, Pallas kernels, packed(): pl.pallas_call(functools.partial(far_kernel, plan, depth), out_shape=(plt...  2.88 us
    pallas_call x1, Pallas kernels, packed(): pl.pallas_call(functools.partial(near_kernel, plan, depth), out_shape=plt...  2.43 us
    pallas_call x1, Pallas kernels, packed(): pl.pallas_call(functools.partial(tail_kernel, plan), out_shape=jax.ShapeD...  1.65 us
  transfers between devices with their start and end apart: 13, of which 7 were waited for; matrix products, arithmetic and copies ran while one was open for 2% of the time, Pallas kernels for 8%

profile of v3, /device:TPU:0, one launch (start us, length us, event | category | flops | bytes accessed | tf_op | source)
XLA Modules:
  0.0 41.9 jit_solution(7748072011549097496)
XLA Ops:
  0.0 2.9 %far.1 = (bf16[2,336,128]{2,1,0:T(8,128)(2,1)S(1)}, bf16[2,48,128]{2,1,0:T(8,128)(2,1)S(1)}, bf16[144,2048]{1,0:T(8,128)(2,1)S(1)}) custom-call(bf16[144,2048]{1,0:T(8,128)(2,1)} %bitcast.38, bf16[16,128]{1,0:T(8,128)(2,1)} %bitcast.39, bf16[2048,1152]{1,0:T(8,128)(2,1)} %w_hbm.4, bf16[256,256]{1,0:T(8,128)(2,1)} %constant.116.clone.table_hbm), custom_call_target="tpu_custom_call" | custom-call | flops 339738624 | bytes 2359296 | tf_op jit(solution)/shard_map/far/pallas_call | solution.py:641
  2.9 0.0 copy-start
  2.9 0.0 copy-start.3
  2.9 2.4 %near.1 = bf16[2,336,128]{2,1,0:T(8,128)(2,1)S(1)} custom-call(bf16[144,2048]{1,0:T(8,128)(2,1)S(1)} %get-tuple-element.12.normed_ref, bf16[2,48,128]{2,1,0:T(8,128)(2,1)S(1)} %get-tuple-element.13.near_ref, bf16[2048,1152]{1,0:T(8,128)(2,1)} %w_hbm.4, bf16[256,256]{1,0:T(8,128)(2,1)} %constant.116.clone.table_hbm), custom_call_target="tpu_custom_call" | custom-call | flops 339738624 | bytes 2359296 | tf_op jit(solution)/shard_map/near/pallas_call | solution.py:662
  5.4 3.1 %collective-permute-start = (bf16[336,128]{1,0:T(8,128)(2,1)S(1)}, bf16[336,128]{1,0:T(8,128)(2,1)S(1)}, u32[]{:S(2)}, u32[]{:S(2)}) collective-permute-start(bf16[336,128]{1,0:T(8,128)(2,1)S(1)} %get-tuple-element.29), channel_id=1, source_target_pairs={{0,8},{8,0},{16,24},{24,16},{1,9},{9,1},{17,25},{25,17},{2,10},{10... | collective-permute-start | bytes 258056 | tf_op jit(solution)/shard_map/ppermute | solution.py:594
  8.5 0.0 copy-start.1
  8.5 0.0 copy-start.2
  8.5 2.5 %collective-permute-start.2 = (bf16[336,128]{1,0:T(8,128)(2,1)S(1)}, bf16[336,128]{1,0:T(8,128)(2,1)S(1)}, u32[]{:S(2)}, u32[]{:S(2)}) collective-permute-start(bf16[336,128]{1,0:T(8,128)(2,1)S(1)} %get-tuple-element.27), channel_id=1, source_target_pairs={{0,24},{8,16},{16,8},{24,0},{1,25},{9,17},{17,9},{25,1},{2,26},{10... | collective-permute-start | bytes 258056 | tf_op jit(solution)/shard_map/ppermute | solution.py:594
  11.1 0.2 collective-permute-start.1
  11.3 0.9 %dynamic-slice_bitcast_fusion.refs_4_ = bf16[9,64,64]{2,1,0:T(8,128)(2,1)S(1)} fusion(bf16[8,9,64,64]{3,2,1,0:T(8,128)(2,1)} %constant.117.clone, s32[]{:T(128)S(6)} %select_n.100), kind=kLoop, calls=%fused_computation.1 | loop fusion | bytes 147460 | tf_op jit(solution)/shard_map/jit(dynamic_index_in_dim)/squeeze | solution.py:678
  12.2 4.0 %collective-permute-done.2.refs_3_ = bf16[336,128]{1,0:T(8,128)(2,1)S(1)} collective-permute-done((bf16[336,128]{1,0:T(8,128)(2,1)S(1)}, bf16[336,128]{1,0:T(8,128)(2,1)S(1)}, u32[]{:S(2)}, u32[]{:S(2)}) %collective-permute-start.2) | collective-permute-done | bytes 86048 | tf_op jit(solution)/shard_map/ppermute | solution.py:594
  16.3 2.8 %collective-permute-done.1.refs_2_ = bf16[336,128]{1,0:T(8,128)(2,1)S(1)} collective-permute-done((bf16[336,128]{1,0:T(8,128)(2,1)S(1)}, bf16[336,128]{1,0:T(8,128)(2,1)S(1)}, u32[]{:S(2)}, u32[]{:S(2)}) %collective-permute-start.1) | collective-permute-done | bytes 86048 | tf_op jit(solution)/shard_map/ppermute | solution.py:594
  19.1 0.3 first.1
  19.5 1.6 %collective-permute-start.6 = (bf16[336,128]{1,0:T(8,128)(2,1)S(1)}, bf16[336,128]{1,0:T(8,128)(2,1)S(1)}, u32[]{:S(2)}, u32[]{:S(2)}) collective-permute-start(bf16[336,128]{1,0:T(8,128)(2,1)S(1)} %pad_maximum_fusion), channel_id=1, source_target_pairs={{0,4},{1,3},{2,6},{3,1},{4,0},{5,7},{6,2},{7,5},{8,12},{9,11},{10,... | collective-permute-start | bytes 258056 | tf_op jit(solution)/shard_map/ppermute | solution.py:614
  21.1 1.4 %collective-permute-start.8 = (bf16[336,128]{1,0:T(8,128)(2,1)S(1)}, bf16[336,128]{1,0:T(8,128)(2,1)S(1)}, u32[]{:S(2)}, u32[]{:S(2)}) collective-permute-start(bf16[336,128]{1,0:T(8,128)(2,1)S(1)} %pad_maximum_fusion.1), channel_id=1, source_target_pairs={{0,6},{1,7},{2,4},{3,5},{4,2},{5,3},{6,0},{7,1},{8,14},{9,15},{10,... | collective-permute-start | bytes 258056 | tf_op jit(solution)/shard_map/ppermute | solution.py:614
  22.5 0.3 collective-permute-start.5
  22.8 0.5 %collective-permute-start.4 = (bf16[168,128]{1,0:T(8,128)(2,1)S(1)}, bf16[168,128]{1,0:T(8,128)(2,1)S(1)}, u32[]{:S(2)}, u32[]{:S(2)}) collective-permute-start(bf16[168,128]{1,0:T(8,128)(2,1)S(1)} %get-tuple-element.24), channel_id=1, source_target_pairs={{0,2},{1,5},{2,0},{3,7},{4,6},{5,1},{6,4},{7,3},{8,10},{9,13},{10,... | collective-permute-start | bytes 129032 | tf_op jit(solution)/shard_map/ppermute | solution.py:614
  23.3 1.0 %collective-permute-start.3 = (bf16[168,128]{1,0:T(8,128)(2,1)S(1)}, bf16[168,128]{1,0:T(8,128)(2,1)S(1)}, u32[]{:S(2)}, u32[]{:S(2)}) collective-permute-start(bf16[168,128]{1,0:T(8,128)(2,1)S(1)} %get-tuple-element.25), channel_id=1, source_target_pairs={{0,1},{1,0},{2,3},{3,2},{4,5},{5,4},{6,7},{7,6},{8,9},{9,8},{10,11... | collective-permute-start | bytes 129032 | tf_op jit(solution)/shard_map/ppermute | solution.py:614
  24.4 0.1 collective-permute-start.7
  24.4 2.1 %collective-permute-done.8.refs_6_ = bf16[336,128]{1,0:T(8,128)(2,1)S(1)} collective-permute-done((bf16[336,128]{1,0:T(8,128)(2,1)S(1)}, bf16[336,128]{1,0:T(8,128)(2,1)S(1)}, u32[]{:S(2)}, u32[]{:S(2)}) %collective-permute-start.8) | collective-permute-done | bytes 86048 | tf_op jit(solution)/shard_map/ppermute | solution.py:614
  26.6 0.1 broadcast_select_fusion.refs_9_.first_ref
  26.6 0.2 collective-permute-done.5.refs_3_
  26.9 0.9 %collective-permute-done.9.refs_7_ = bf16[168,128]{1,0:T(8,128)(2,1)S(1)} collective-permute-done((bf16[168,128]{1,0:T(8,128)(2,1)S(1)}, bf16[168,128]{1,0:T(8,128)(2,1)S(1)}, u32[]{:S(2)}, u32[]{:S(2)}) %collective-permute-start.9) | collective-permute-done | bytes 43040 | tf_op jit(solution)/shard_map/ppermute | solution.py:614
  27.8 0.6 %second_far.1 = (bf16[2,328,128]{2,1,0:T(8,128)(2,1)S(1)}, bf16[2,288,384]{2,1,0:T(8,128)(2,1)S(1)}) custom-call(bf16[168,128]{1,0:T(8,128)(2,1)S(1)} %get-tuple-element.26.refs_0_, bf16[168,128]{1,0:T(8,128)(2,1)S(1)} %collective-permute-done.3.refs_1_, bf16[168,128]{1,0:T(8,128)(2,1)S(1)} %collective-permute-done.4.refs_2_, ...), custom_call_target="tpu_custom_call" | custom-call | flops 300000000 | bytes 1000000 | tf_op jit(solution)/shard_map/second_far/pallas_call | solution.py:696
  28.4 0.5 %second_near.1 = bf16[2,328,128]{2,1,0:T(8,128)(2,1)S(1)} custom-call(bf16[576,288]{1,0:T(8,128)(2,1)S(1)} %copy-done, bf16[576,288]{1,0:T(8,128)(2,1)S(1)} %broadcast_select_fusion.refs_9_.first_ref, bf16[2,288,384]{2,1,0:T(8,128)(2,1)S(1)} %get-tuple-element.15.rhs_ref), custom_call_target="tpu_custom_call" | custom-call | flops 300000000 | bytes 1000000 | tf_op jit(solution)/shard_map/second_near/pallas_call | solution.py:706
  28.9 0.1 collective-permute-start.10
  29.0 2.6 %collective-permute-start.12 = (bf16[328,128]{1,0:T(8,128)(2,1)S(1)}, bf16[328,128]{1,0:T(8,128)(2,1)S(1)}, u32[]{:S(2)}, u32[]{:S(2)}) collective-permute-start(bf16[328,128]{1,0:T(8,128)(2,1)S(1)} %get-tuple-element.31), channel_id=1, source_target_pairs={{0,24},{8,16},{16,8},{24,0},{1,25},{9,17},{17,9},{25,1},{2,26},{10... | collective-permute-start | bytes 251912 | tf_op jit(solution)/shard_map/ppermute | solution.py:594
  31.6 0.9 %collective-permute-start.11 = (bf16[328,128]{1,0:T(8,128)(2,1)S(1)}, bf16[328,128]{1,0:T(8,128)(2,1)S(1)}, u32[]{:S(2)}, u32[]{:S(2)}) collective-permute-start(bf16[328,128]{1,0:T(8,128)(2,1)S(1)} %get-tuple-element.32), channel_id=1, source_target_pairs={{0,16},{8,24},{16,0},{24,8},{1,17},{9,25},{17,1},{25,9},{2,18},{10... | collective-permute-start | bytes 251912 | tf_op jit(solution)/shard_map/ppermute | solution.py:594
  32.6 3.2 %early.1 = (f32[144,2048]{1,0:T(8,128)S(1)}, bf16[896,2048]{1,0:T(8,128)(2,1)S(1)}) custom-call(bf16[328,128]{1,0:T(8,128)(2,1)S(1)} %get-tuple-element.34.slab_ref.refs_0_, bf16[256,256]{1,0:T(8,128)(2,1)S(1)} %copy-done.2, bf16[144,144]{1,0:T(8,128)(2,1)S(1)} %copy-done.1, bf16[1152,2048]{1,0:T(8,128)(2,1)} %w_hbm.5), custom_call_target="tpu_custom_call" | custom-call | flops 339738624 | bytes 2359296 | tf_op jit(solution)/shard_map/early/pallas_call | solution.py:720
  35.8 0.9 %collective-permute-done.12.refs_3_ = bf16[328,128]{1,0:T(8,128)(2,1)S(1)} collective-permute-done((bf16[328,128]{1,0:T(8,128)(2,1)S(1)}, bf16[328,128]{1,0:T(8,128)(2,1)S(1)}, u32[]{:S(2)}, u32[]{:S(2)}) %collective-permute-start.12) | collective-permute-done | bytes 84000 | tf_op jit(solution)/shard_map/ppermute | solution.py:594
  36.8 3.5 %collective-permute-done.11.refs_2_ = bf16[328,128]{1,0:T(8,128)(2,1)S(1)} collective-permute-done((bf16[328,128]{1,0:T(8,128)(2,1)S(1)}, bf16[328,128]{1,0:T(8,128)(2,1)S(1)}, u32[]{:S(2)}, u32[]{:S(2)}) %collective-permute-start.11) | collective-permute-done | bytes 84000 | tf_op jit(solution)/shard_map/ppermute | solution.py:594
  40.2 1.6 %tail.1 = bf16[36,4,2048]{2,1,0:T(4,128)(2,1)} custom-call(bf16[328,128]{1,0:T(8,128)(2,1)S(1)} %get-tuple-element.34.slab_ref.refs_0_, bf16[328,128]{1,0:T(8,128)(2,1)S(1)} %collective-permute-done.10.refs_1_, bf16[328,128]{1,0:T(8,128)(2,1)S(1)} %collective-permute-done.11.refs_2_, bf16[328,128]{1,0:T(8,128)(2,1)S(1)} %collective-permute-done.12.refs_3_, ...), custom_call_target="tpu_custom_call" | custom-call | flops 339738624 | bytes 2359296 | tf_op jit(solution)/shard_map/tail/pallas_call | solution.py:737
  (20 shorter events, 0.2 us)
Async XLA Ops:
  2.9 23.7 %copy-start = (bf16[576,288]{1,0:T(8,128)(2,1)S(1)}, bf16[576,288]{1,0:T(8,128)(2,1)}, u32[]{:S(2)}) copy-start(bf16[576,288]{1,0:T(8,128)(2,1)} %constant.123.refs_8_.usual_ref) | copy-start | bytes 995332
  2.9 23.7 %copy-start.3 = (bf16[576,288]{1,0:T(8,128)(2,1)S(1)}, bf16[576,288]{1,0:T(8,128)(2,1)}, u32[]{:S(2)}) copy-start(bf16[576,288]{1,0:T(8,128)(2,1)} %constant.124) | copy-start | bytes 995332
  5.4 6.8 %collective-permute-start = (bf16[336,128]{1,0:T(8,128)(2,1)S(1)}, bf16[336,128]{1,0:T(8,128)(2,1)S(1)}, u32[]{:S(2)}, u32[]{:S(2)}) collective-permute-start(bf16[336,128]{1,0:T(8,128)(2,1)S(1)} %get-tuple-element.29), channel_id=1, source_target_pairs={{0,8},{8,0},{16,24},{24,16},{1,9},{9,1},{17,25},{25,17},{2,10},{10... | collective-permute-start | bytes 258056 | tf_op jit(solution)/shard_map/ppermute | solution.py:594
  8.5 24.0 %copy-start.1 = (bf16[144,144]{1,0:T(8,128)(2,1)S(1)}, bf16[144,144]{1,0:T(8,128)(2,1)}, u32[]{:S(2)}) copy-start(bf16[144,144]{1,0:T(8,128)(2,1)} %constant.121.clone.order_ref.refs_4_) | copy-start | bytes 124420
  8.5 24.0 %copy-start.2 = (bf16[256,256]{1,0:T(8,128)(2,1)S(1)}, bf16[256,256]{1,0:T(8,128)(2,1)}, u32[]{:S(2)}) copy-start(bf16[256,256]{1,0:T(8,128)(2,1)} %constant.120.clone.unfold_ref) | copy-start | bytes 393220
  8.5 7.7 %collective-permute-start.2 = (bf16[336,128]{1,0:T(8,128)(2,1)S(1)}, bf16[336,128]{1,0:T(8,128)(2,1)S(1)}, u32[]{:S(2)}, u32[]{:S(2)}) collective-permute-start(bf16[336,128]{1,0:T(8,128)(2,1)S(1)} %get-tuple-element.27), channel_id=1, source_target_pairs={{0,24},{8,16},{16,8},{24,0},{1,25},{9,17},{17,9},{25,1},{2,26},{10... | collective-permute-start | bytes 258056 | tf_op jit(solution)/shard_map/ppermute | solution.py:594
  11.1 8.0 %collective-permute-start.1 = (bf16[336,128]{1,0:T(8,128)(2,1)S(1)}, bf16[336,128]{1,0:T(8,128)(2,1)S(1)}, u32[]{:S(2)}, u32[]{:S(2)}) collective-permute-start(bf16[336,128]{1,0:T(8,128)(2,1)S(1)} %get-tuple-element.28), channel_id=1, source_target_pairs={{0,16},{8,24},{16,0},{24,8},{1,17},{9,25},{17,1},{25,9},{2,18},{10... | collective-permute-start | bytes 258056 | tf_op jit(solution)/shard_map/ppermute | solution.py:594
  19.5 4.9 %collective-permute-start.6 = (bf16[336,128]{1,0:T(8,128)(2,1)S(1)}, bf16[336,128]{1,0:T(8,128)(2,1)S(1)}, u32[]{:S(2)}, u32[]{:S(2)}) collective-permute-start(bf16[336,128]{1,0:T(8,128)(2,1)S(1)} %pad_maximum_fusion), channel_id=1, source_target_pairs={{0,4},{1,3},{2,6},{3,1},{4,0},{5,7},{6,2},{7,5},{8,12},{9,11},{10,... | collective-permute-start | bytes 258056 | tf_op jit(solution)/shard_map/ppermute | solution.py:614
  21.1 5.5 %collective-permute-start.8 = (bf16[336,128]{1,0:T(8,128)(2,1)S(1)}, bf16[336,128]{1,0:T(8,128)(2,1)S(1)}, u32[]{:S(2)}, u32[]{:S(2)}) collective-permute-start(bf16[336,128]{1,0:T(8,128)(2,1)S(1)} %pad_maximum_fusion.1), channel_id=1, source_target_pairs={{0,6},{1,7},{2,4},{3,5},{4,2},{5,3},{6,0},{7,1},{8,14},{9,15},{10,... | collective-permute-start | bytes 258056 | tf_op jit(solution)/shard_map/ppermute | solution.py:614
  22.5 4.4 %collective-permute-start.5 = (bf16[168,128]{1,0:T(8,128)(2,1)S(1)}, bf16[168,128]{1,0:T(8,128)(2,1)S(1)}, u32[]{:S(2)}, u32[]{:S(2)}) collective-permute-start(bf16[168,128]{1,0:T(8,128)(2,1)S(1)} %get-tuple-element.23), channel_id=1, source_target_pairs={{0,3},{1,4},{2,1},{3,6},{4,7},{5,0},{6,5},{7,2},{8,11},{9,12},{10,... | collective-permute-start | bytes 129032 | tf_op jit(solution)/shard_map/ppermute | solution.py:614
  22.8 4.1 %collective-permute-start.4 = (bf16[168,128]{1,0:T(8,128)(2,1)S(1)}, bf16[168,128]{1,0:T(8,128)(2,1)S(1)}, u32[]{:S(2)}, u32[]{:S(2)}) collective-permute-start(bf16[168,128]{1,0:T(8,128)(2,1)S(1)} %get-tuple-element.24), channel_id=1, source_target_pairs={{0,2},{1,5},{2,0},{3,7},{4,6},{5,1},{6,4},{7,3},{8,10},{9,13},{10,... | collective-permute-start | bytes 129032 | tf_op jit(solution)/shard_map/ppermute | solution.py:614
  23.3 3.5 %collective-permute-start.3 = (bf16[168,128]{1,0:T(8,128)(2,1)S(1)}, bf16[168,128]{1,0:T(8,128)(2,1)S(1)}, u32[]{:S(2)}, u32[]{:S(2)}) collective-permute-start(bf16[168,128]{1,0:T(8,128)(2,1)S(1)} %get-tuple-element.25), channel_id=1, source_target_pairs={{0,1},{1,0},{2,3},{3,2},{4,5},{5,4},{6,7},{7,6},{8,9},{9,8},{10,11... | collective-permute-start | bytes 129032 | tf_op jit(solution)/shard_map/ppermute | solution.py:614
  24.4 2.5 %collective-permute-start.7 = (bf16[168,128]{1,0:T(8,128)(2,1)S(1)}, bf16[168,128]{1,0:T(8,128)(2,1)S(1)}, u32[]{:S(2)}, u32[]{:S(2)}) collective-permute-start(bf16[168,128]{1,0:T(8,128)(2,1)S(1)} %slice.8), channel_id=1, source_target_pairs={{0,1},{1,0},{2,3},{3,2},{4,5},{5,4},{6,7},{7,6},{8,9},{9,8},{10,11... | collective-permute-start | bytes 129032 | tf_op jit(solution)/shard_map/ppermute | solution.py:614
  26.6 1.2 %collective-permute-start.9 = (bf16[168,128]{1,0:T(8,128)(2,1)S(1)}, bf16[168,128]{1,0:T(8,128)(2,1)S(1)}, u32[]{:S(2)}, u32[]{:S(2)}) collective-permute-start(bf16[168,128]{1,0:T(8,128)(2,1)S(1)} %slice.9), channel_id=1, source_target_pairs={{0,1},{1,0},{2,3},{3,2},{4,5},{5,4},{6,7},{7,6},{8,9},{9,8},{10,11... | collective-permute-start | bytes 129032 | tf_op jit(solution)/shard_map/ppermute | solution.py:614
  28.9 6.9 %collective-permute-start.10 = (bf16[328,128]{1,0:T(8,128)(2,1)S(1)}, bf16[328,128]{1,0:T(8,128)(2,1)S(1)}, u32[]{:S(2)}, u32[]{:S(2)}) collective-permute-start(bf16[328,128]{1,0:T(8,128)(2,1)S(1)} %get-tuple-element.33), channel_id=1, source_target_pairs={{0,8},{8,0},{16,24},{24,16},{1,9},{9,1},{17,25},{25,17},{2,10},{10... | collective-permute-start | bytes 251912 | tf_op jit(solution)/shard_map/ppermute | solution.py:594
  29.0 7.7 %collective-permute-start.12 = (bf16[328,128]{1,0:T(8,128)(2,1)S(1)}, bf16[328,128]{1,0:T(8,128)(2,1)S(1)}, u32[]{:S(2)}, u32[]{:S(2)}) collective-permute-start(bf16[328,128]{1,0:T(8,128)(2,1)S(1)} %get-tuple-element.31), channel_id=1, source_target_pairs={{0,24},{8,16},{16,8},{24,0},{1,25},{9,17},{17,9},{25,1},{2,26},{10... | collective-permute-start | bytes 251912 | tf_op jit(solution)/shard_map/ppermute | solution.py:594
  31.6 8.6 %collective-permute-start.11 = (bf16[328,128]{1,0:T(8,128)(2,1)S(1)}, bf16[328,128]{1,0:T(8,128)(2,1)S(1)}, u32[]{:S(2)}, u32[]{:S(2)}) collective-permute-start(bf16[328,128]{1,0:T(8,128)(2,1)S(1)} %get-tuple-element.32), channel_id=1, source_target_pairs={{0,16},{8,24},{16,0},{24,8},{1,17},{9,25},{17,1},{25,9},{2,18},{10... | collective-permute-start | bytes 251912 | tf_op jit(solution)/shard_map/ppermute | solution.py:594

commit v4 on v3

--- a/solution.py
+++ b/solution.py
@@ -124,8 +124,8 @@
 
 LANES = 128
 TILE = 8
-STEPS = 1
-WIDE = 256
+STEPS = 2
+WIDE = 512
 RELAYED = ((0, 0), (1, 1), (2, 4), (5, 3), (4, 2), (3, 5), (6, 6), (7, 7))
 VMEM = pl.BlockSpec(memory_space=pltpu.VMEM)
 HBM = pl.BlockSpec(memory_space=pltpu.HBM)
@@ -499,6 +499,10 @@
     return dot(ordered, unfold).astype(jnp.bfloat16)
 
 
+def arrivals(rows):
+    return [rows - 1, *range(1, rows - 1)]
+
+
 def early_kernel(plan, slab_ref, unfold_ref, order_ref, w_hbm, partial_ref, w_ref, own_ref, raw_ref, sems):
     row = lax.axis_index("row")
     each = plan.full * GROUP
@@ -507,8 +511,8 @@
         return w_hbm.at[pl.ds(pl.multiple_of((row ^ s) * each, LANES), each), :]
 
     copies = [pltpu.make_async_copy(part(0), own_ref, sems.at[0])]
-    for s in range(1, plan.rows):
-        copies.append(pltpu.make_async_copy(part(s), raw_ref.at[pl.ds((s - 1) * each, each), :], sems.at[s]))
+    for n, s in enumerate(arrivals(plan.rows)):
+        copies.append(pltpu.make_async_copy(part(s), raw_ref.at[pl.ds(n * each, each), :], sems.at[s]))
     copies.append(
         pltpu.make_async_copy(
             w_hbm.at[pl.ds(plan.rows * each, GROUP), :],
@@ -533,6 +537,14 @@
             w_ref[rows, columns] = dot(unfold[:size, :size], raw_ref[rows, columns]).astype(jnp.bfloat16)
 
 
+def middle_kernel(plan, slab_ref, order_ref, w_ref, partial_ref, out_ref):
+    pair = [slab_ref[f * plan.out_rows : (f + 1) * plan.out_rows, :] for f in range(plan.full)]
+    ordered = dot(order_ref[...], jnp.concatenate(pair, axis=1)).astype(jnp.bfloat16)
+    for n in range(plan.features // 512):
+        columns = slice(n * 512, (n + 1) * 512)
+        out_ref[:, columns] = partial_ref[:, columns] + dot(ordered, w_ref[: plan.full * GROUP, columns])
+
+
 def tail_kernel(plan, *refs):
     slabs = refs[: plan.rows]
     order_ref, partial_ref, w_ref, out_hbm, packed_ref, stage_ref, sems = refs[plan.rows :]
@@ -550,7 +562,7 @@
             by_lane([turned[q][(q - inner) % plan.rows][rows, :] for q in range(plan.rows)], plan.sub)
         )
     parts = []
-    for s in range(1, plan.rows):
+    for s in arrivals(plan.rows)[1:]:
         parts += [slabs[s][f * plan.out_rows : (f + 1) * plan.out_rows, :] for f in range(plan.full)]
     parts.append(jnp.concatenate(pieces, axis=0).astype(jnp.bfloat16))
     ordered = dot(order_ref[...], jnp.concatenate(parts, axis=1)).astype(jnp.bfloat16)
@@ -558,7 +570,7 @@
     copies = []
     for n in range(plan.features // WIDE):
         columns = slice(n * WIDE, (n + 1) * WIDE)
-        result = (partial_ref[:, columns] + dot(ordered, w_ref[:, columns])).astype(jnp.bfloat16)
+        result = (partial_ref[:, columns] + dot(ordered, w_ref[plan.full * GROUP :, columns])).astype(jnp.bfloat16)
         for k in range(plan.block_b):
             stage_ref[n, k] = result[k * group : (k + 1) * group, :]
         copy = pltpu.make_async_copy(stage_ref.at[n], out_hbm.at[:, :, pl.ds(n * WIDE, WIDE)], sems.at[n])
@@ -734,6 +746,15 @@
         cost_estimate=cost,
         name="early",
     )(slabs[0], unfold, order, pltpu.with_memory_space_constraint(w_out, pltpu.HBM))
+    partial = pl.pallas_call(
+        functools.partial(middle_kernel, plan),
+        out_shape=pltpu.VMEM((plan.out_rows, features), jnp.float32),
+        in_specs=[VMEM] * 4,
+        out_specs=VMEM,
+        compiler_params=limit(8),
+        cost_estimate=estimate(10**8, 10**6),
+        name="middle",
+    )(slabs[plan.rows - 1], order, w_rest, partial)
     return pl.pallas_call(
         functools.partial(tail_kernel, plan),
         out_shape=jax.ShapeDtypeStruct((plan.block_b, 2 * plan.pairs, features), half_type),

time: 42.1 us -> 40.7 us (0.967)
  waiting for transfers between devices: 14.5 us -> 12.1 us
  starting transfers between devices: 14.4 us -> 15.3 us
    ppermute x6, waiting for transfers between devices: 11.3 us -> 8.82 us  [exchange(): slab = lax.ppermute(slab, axis, [(n, n ^ s) for n in range(size)])]
    ppermute x6, starting transfers between devices: 9.46 us -> 10.3 us  [exchange(): slab = lax.ppermute(slab, axis, [(n, n ^ s) for n in range(size)])]
    pallas_call x0 -> x1, Pallas kernels: none -> 0.44 us  [packed(): pl.pallas_call(functools.partial(middle_kernel, plan), out_shape=pltpu.VM...]
  transfers between devices with their start and end apart: 13 -> 13, of which waited for: 7 -> 7; matrix products, arithmetic and copies ran while one was open for 2% -> 3% of each run, Pallas kernels for 8% -> 9%
where the time goes in v4:
time: 40.7 us; the launch traced here: 40.6 us
  starting transfers between devices  15.3 us (38%)
  waiting for transfers between devices  12.1 us (30%)
  Pallas kernels  11.8 us (29%)
  local copies, waits for them, and re-layouts  1.14 us (3%)
    ppermute x6, starting transfers between devices, exchange(): slab = lax.ppermute(slab, axis, [(n, n ^ s) for n in range(size)])  10.3 us
    ppermute x6, waiting for transfers between devices, exchange(): slab = lax.ppermute(slab, axis, [(n, n ^ s) for n in range(size)])  8.82 us
    ppermute x7, starting transfers between devices, send(): lax.ppermute(value, 'col', [(n, n ^ pair[n % 2]) for n in range(cols)])  4.96 us
    pallas_call x1, Pallas kernels, packed(): pl.pallas_call(functools.partial(early_kernel, plan), out_shape=(pltpu.VM...  3.25 us
    ppermute x7, waiting for transfers between devices, send(): lax.ppermute(value, 'col', [(n, n ^ pair[n % 2]) for n in range(cols)])  3.24 us
    pallas_call x1, Pallas kernels, packed(): pl.pallas_call(functools.partial(far_kernel, plan, depth), out_shape=(plt...  2.89 us
    pallas_call x1, Pallas kernels, packed(): pl.pallas_call(functools.partial(near_kernel, plan, depth), out_shape=plt...  2.35 us
    pallas_call x1, Pallas kernels, packed(): pl.pallas_call(functools.partial(tail_kernel, plan), out_shape=jax.ShapeD...  1.47 us
  transfers between devices with their start and end apart: 13, of which 7 were waited for; matrix products, arithmetic and copies ran while one was open for 3% of the time, Pallas kernels for 9%

profile of v4, /device:TPU:0, one launch (start us, length us, event | category | flops | bytes accessed | tf_op | source)
XLA Modules:
  0.0 40.6 jit_solution(10850292662136913086)
XLA Ops:
  0.0 2.9 %far.1 = (bf16[2,336,128]{2,1,0:T(8,128)(2,1)S(1)}, bf16[2,48,128]{2,1,0:T(8,128)(2,1)S(1)}, bf16[144,2048]{1,0:T(8,128)(2,1)S(1)}) custom-call(bf16[144,2048]{1,0:T(8,128)(2,1)} %bitcast.38, bf16[16,128]{1,0:T(8,128)(2,1)} %bitcast.39, bf16[2048,1152]{1,0:T(8,128)(2,1)} %w_hbm.4, bf16[256,256]{1,0:T(8,128)(2,1)} %constant.116.clone.table_hbm), custom_call_target="tpu_custom_call" | custom-call | flops 339738624 | bytes 2359296 | tf_op jit(solution)/shard_map/far/pallas_call | solution.py:653
  2.9 2.3 %near.1 = bf16[2,336,128]{2,1,0:T(8,128)(2,1)S(1)} custom-call(bf16[144,2048]{1,0:T(8,128)(2,1)S(1)} %get-tuple-element.12.normed_ref, bf16[2,48,128]{2,1,0:T(8,128)(2,1)S(1)} %get-tuple-element.13.near_ref, bf16[2048,1152]{1,0:T(8,128)(2,1)} %w_hbm.4, bf16[256,256]{1,0:T(8,128)(2,1)} %constant.116.clone.table_hbm), custom_call_target="tpu_custom_call" | custom-call | flops 339738624 | bytes 2359296 | tf_op jit(solution)/shard_map/near/pallas_call | solution.py:674
  5.3 3.1 %collective-permute-start = (bf16[336,128]{1,0:T(8,128)(2,1)S(1)}, bf16[336,128]{1,0:T(8,128)(2,1)S(1)}, u32[]{:S(2)}, u32[]{:S(2)}) collective-permute-start(bf16[336,128]{1,0:T(8,128)(2,1)S(1)} %get-tuple-element.29), channel_id=1, source_target_pairs={{0,8},{8,0},{16,24},{24,16},{1,9},{9,1},{17,25},{25,17},{2,10},{10... | collective-permute-start | bytes 258056 | tf_op jit(solution)/shard_map/ppermute | solution.py:606
  8.4 2.6 %collective-permute-start.2 = (bf16[336,128]{1,0:T(8,128)(2,1)S(1)}, bf16[336,128]{1,0:T(8,128)(2,1)S(1)}, u32[]{:S(2)}, u32[]{:S(2)}) collective-permute-start(bf16[336,128]{1,0:T(8,128)(2,1)S(1)} %get-tuple-element.27), channel_id=1, source_target_pairs={{0,24},{8,16},{16,8},{24,0},{1,25},{9,17},{17,9},{25,1},{2,26},{10... | collective-permute-start | bytes 258056 | tf_op jit(solution)/shard_map/ppermute | solution.py:606
  11.0 0.2 collective-permute-start.1
  11.1 1.0 %dynamic-slice_bitcast_fusion.refs_4_ = bf16[9,64,64]{2,1,0:T(8,128)(2,1)S(1)} fusion(bf16[8,9,64,64]{3,2,1,0:T(8,128)(2,1)} %constant.117.clone, s32[]{:T(128)S(6)} %select_n.100), kind=kLoop, calls=%fused_computation.1 | loop fusion | bytes 147460 | tf_op jit(solution)/shard_map/jit(dynamic_index_in_dim)/squeeze | solution.py:690
  12.1 0.0 collective-permute-done.refs_1_
  12.2 4.0 %collective-permute-done.2.refs_3_ = bf16[336,128]{1,0:T(8,128)(2,1)S(1)} collective-permute-done((bf16[336,128]{1,0:T(8,128)(2,1)S(1)}, bf16[336,128]{1,0:T(8,128)(2,1)S(1)}, u32[]{:S(2)}, u32[]{:S(2)}) %collective-permute-start.2) | collective-permute-done | bytes 86048 | tf_op jit(solution)/shard_map/ppermute | solution.py:606
  16.2 2.8 %collective-permute-done.1.refs_2_ = bf16[336,128]{1,0:T(8,128)(2,1)S(1)} collective-permute-done((bf16[336,128]{1,0:T(8,128)(2,1)S(1)}, bf16[336,128]{1,0:T(8,128)(2,1)S(1)}, u32[]{:S(2)}, u32[]{:S(2)}) %collective-permute-start.1) | collective-permute-done | bytes 86048 | tf_op jit(solution)/shard_map/ppermute | solution.py:606
  19.0 0.3 first.1
  19.3 1.6 %collective-permute-start.6 = (bf16[336,128]{1,0:T(8,128)(2,1)S(1)}, bf16[336,128]{1,0:T(8,128)(2,1)S(1)}, u32[]{:S(2)}, u32[]{:S(2)}) collective-permute-start(bf16[336,128]{1,0:T(8,128)(2,1)S(1)} %pad_maximum_fusion), channel_id=1, source_target_pairs={{0,4},{1,3},{2,6},{3,1},{4,0},{5,7},{6,2},{7,5},{8,12},{9,11},{10,... | collective-permute-start | bytes 258056 | tf_op jit(solution)/shard_map/ppermute | solution.py:626
  20.9 1.4 %collective-permute-start.8 = (bf16[336,128]{1,0:T(8,128)(2,1)S(1)}, bf16[336,128]{1,0:T(8,128)(2,1)S(1)}, u32[]{:S(2)}, u32[]{:S(2)}) collective-permute-start(bf16[336,128]{1,0:T(8,128)(2,1)S(1)} %pad_maximum_fusion.1), channel_id=1, source_target_pairs={{0,6},{1,7},{2,4},{3,5},{4,2},{5,3},{6,0},{7,1},{8,14},{9,15},{10,... | collective-permute-start | bytes 258056 | tf_op jit(solution)/shard_map/ppermute | solution.py:626
  22.4 0.3 collective-permute-start.5
  22.7 0.5 %collective-permute-start.4 = (bf16[168,128]{1,0:T(8,128)(2,1)S(1)}, bf16[168,128]{1,0:T(8,128)(2,1)S(1)}, u32[]{:S(2)}, u32[]{:S(2)}) collective-permute-start(bf16[168,128]{1,0:T(8,128)(2,1)S(1)} %get-tuple-element.24), channel_id=1, source_target_pairs={{0,2},{1,5},{2,0},{3,7},{4,6},{5,1},{6,4},{7,3},{8,10},{9,13},{10,... | collective-permute-start | bytes 129032 | tf_op jit(solution)/shard_map/ppermute | solution.py:626
  23.2 1.0 %collective-permute-start.3 = (bf16[168,128]{1,0:T(8,128)(2,1)S(1)}, bf16[168,128]{1,0:T(8,128)(2,1)S(1)}, u32[]{:S(2)}, u32[]{:S(2)}) collective-permute-start(bf16[168,128]{1,0:T(8,128)(2,1)S(1)} %get-tuple-element.25), channel_id=1, source_target_pairs={{0,1},{1,0},{2,3},{3,2},{4,5},{5,4},{6,7},{7,6},{8,9},{9,8},{10,11... | collective-permute-start | bytes 129032 | tf_op jit(solution)/shard_map/ppermute | solution.py:626
  24.2 0.1 collective-permute-start.7
  24.3 2.1 %collective-permute-done.8.refs_6_ = bf16[336,128]{1,0:T(8,128)(2,1)S(1)} collective-permute-done((bf16[336,128]{1,0:T(8,128)(2,1)S(1)}, bf16[336,128]{1,0:T(8,128)(2,1)S(1)}, u32[]{:S(2)}, u32[]{:S(2)}) %collective-permute-start.8) | collective-permute-done | bytes 86048 | tf_op jit(solution)/shard_map/ppermute | solution.py:626
  26.5 0.1 broadcast_select_fusion.refs_9_.first_ref
  26.5 0.2 collective-permute-done.5.refs_3_
  26.8 0.9 %collective-permute-done.9.refs_7_ = bf16[168,128]{1,0:T(8,128)(2,1)S(1)} collective-permute-done((bf16[168,128]{1,0:T(8,128)(2,1)S(1)}, bf16[168,128]{1,0:T(8,128)(2,1)S(1)}, u32[]{:S(2)}, u32[]{:S(2)}) %collective-permute-start.9) | collective-permute-done | bytes 43040 | tf_op jit(solution)/shard_map/ppermute | solution.py:626
  27.7 0.6 %second_far.1 = (bf16[2,328,128]{2,1,0:T(8,128)(2,1)S(1)}, bf16[2,288,384]{2,1,0:T(8,128)(2,1)S(1)}) custom-call(bf16[168,128]{1,0:T(8,128)(2,1)S(1)} %get-tuple-element.26.refs_0_, bf16[168,128]{1,0:T(8,128)(2,1)S(1)} %collective-permute-done.3.refs_1_, bf16[168,128]{1,0:T(8,128)(2,1)S(1)} %collective-permute-done.4.refs_2_, ...), custom_call_target="tpu_custom_call" | custom-call | flops 300000000 | bytes 1000000 | tf_op jit(solution)/shard_map/second_far/pallas_call | solution.py:708
  28.3 0.0 copy-start.1
  28.3 0.0 copy-start.2
  28.3 0.5 %second_near.1 = bf16[2,328,128]{2,1,0:T(8,128)(2,1)S(1)} custom-call(bf16[576,288]{1,0:T(8,128)(2,1)S(1)} %copy-done, bf16[576,288]{1,0:T(8,128)(2,1)S(1)} %broadcast_select_fusion.refs_9_.first_ref, bf16[2,288,384]{2,1,0:T(8,128)(2,1)S(1)} %get-tuple-element.15.rhs_ref), custom_call_target="tpu_custom_call" | custom-call | flops 300000000 | bytes 1000000 | tf_op jit(solution)/shard_map/second_near/pallas_call | solution.py:718
  28.8 2.6 %collective-permute-start.12 = (bf16[328,128]{1,0:T(8,128)(2,1)S(1)}, bf16[328,128]{1,0:T(8,128)(2,1)S(1)}, u32[]{:S(2)}, u32[]{:S(2)}) collective-permute-start(bf16[328,128]{1,0:T(8,128)(2,1)S(1)} %get-tuple-element.31), channel_id=1, source_target_pairs={{0,24},{8,16},{16,8},{24,0},{1,25},{9,17},{17,9},{25,1},{2,26},{10... | collective-permute-start | bytes 251912 | tf_op jit(solution)/shard_map/ppermute | solution.py:606
  31.4 0.1 collective-permute-start.10
  31.5 1.9 %collective-permute-start.11 = (bf16[328,128]{1,0:T(8,128)(2,1)S(1)}, bf16[328,128]{1,0:T(8,128)(2,1)S(1)}, u32[]{:S(2)}, u32[]{:S(2)}) collective-permute-start(bf16[328,128]{1,0:T(8,128)(2,1)S(1)} %get-tuple-element.32), channel_id=1, source_target_pairs={{0,16},{8,24},{16,0},{24,8},{1,17},{9,25},{17,1},{25,9},{2,18},{10... | collective-permute-start | bytes 251912 | tf_op jit(solution)/shard_map/ppermute | solution.py:606
  33.4 3.2 %early.1 = (f32[144,2048]{1,0:T(8,128)S(1)}, bf16[896,2048]{1,0:T(8,128)(2,1)S(1)}) custom-call(bf16[328,128]{1,0:T(8,128)(2,1)S(1)} %get-tuple-element.34.slab_ref.refs_0_, bf16[256,256]{1,0:T(8,128)(2,1)S(1)} %copy-done.2, bf16[144,144]{1,0:T(8,128)(2,1)S(1)} %copy-done.1, bf16[1152,2048]{1,0:T(8,128)(2,1)} %w_hbm.5), custom_call_target="tpu_custom_call" | custom-call | flops 339738624 | bytes 2359296 | tf_op jit(solution)/shard_map/early/pallas_call | solution.py:732
  36.6 0.4 %middle.1.refs_5_ = f32[144,2048]{1,0:T(8,128)S(1)} custom-call(bf16[328,128]{1,0:T(8,128)(2,1)S(1)} %collective-permute-done.12.slab_ref.refs_3_, bf16[144,144]{1,0:T(8,128)(2,1)S(1)} %copy-done.1, bf16[896,2048]{1,0:T(8,128)(2,1)S(1)} %get-tuple-element.17.w_ref.refs_6_, f32[144,2048]{1,0:T(8,128)S(1)} %get-tuple-element.18.partial_ref), custom_call_target="tpu_custom_call" | custom-call | flops 100000000 | bytes 1000000 | tf_op jit(solution)/shard_map/middle/pallas_call | solution.py:749
  37.1 1.6 %collective-permute-done.10.refs_1_ = bf16[328,128]{1,0:T(8,128)(2,1)S(1)} collective-permute-done((bf16[328,128]{1,0:T(8,128)(2,1)S(1)}, bf16[328,128]{1,0:T(8,128)(2,1)S(1)}, u32[]{:S(2)}, u32[]{:S(2)}) %collective-permute-start.10) | collective-permute-done | bytes 84000 | tf_op jit(solution)/shard_map/ppermute | solution.py:606
  38.7 0.4 %collective-permute-done.11.refs_2_ = bf16[328,128]{1,0:T(8,128)(2,1)S(1)} collective-permute-done((bf16[328,128]{1,0:T(8,128)(2,1)S(1)}, bf16[328,128]{1,0:T(8,128)(2,1)S(1)}, u32[]{:S(2)}, u32[]{:S(2)}) %collective-permute-start.11) | collective-permute-done | bytes 84000 | tf_op jit(solution)/shard_map/ppermute | solution.py:606
  39.1 1.5 %tail.1 = bf16[36,4,2048]{2,1,0:T(4,128)(2,1)} custom-call(bf16[328,128]{1,0:T(8,128)(2,1)S(1)} %get-tuple-element.34.slab_ref.refs_0_, bf16[328,128]{1,0:T(8,128)(2,1)S(1)} %collective-permute-done.10.refs_1_, bf16[328,128]{1,0:T(8,128)(2,1)S(1)} %collective-permute-done.11.refs_2_, bf16[328,128]{1,0:T(8,128)(2,1)S(1)} %collective-permute-done.12.slab_ref.refs_3_, ...), custom_call_target="tpu_custom_call" | custom-call | flops 339738624 | bytes 2359296 | tf_op jit(solution)/shard_map/tail/pallas_call | solution.py:758
  (21 shorter events, 0.2 us)
Async XLA Ops:
  5.3 6.9 %collective-permute-start = (bf16[336,128]{1,0:T(8,128)(2,1)S(1)}, bf16[336,128]{1,0:T(8,128)(2,1)S(1)}, u32[]{:S(2)}, u32[]{:S(2)}) collective-permute-start(bf16[336,128]{1,0:T(8,128)(2,1)S(1)} %get-tuple-element.29), channel_id=1, source_target_pairs={{0,8},{8,0},{16,24},{24,16},{1,9},{9,1},{17,25},{25,17},{2,10},{10... | collective-permute-start | bytes 258056 | tf_op jit(solution)/shard_map/ppermute | solution.py:606
  8.4 7.8 %collective-permute-start.2 = (bf16[336,128]{1,0:T(8,128)(2,1)S(1)}, bf16[336,128]{1,0:T(8,128)(2,1)S(1)}, u32[]{:S(2)}, u32[]{:S(2)}) collective-permute-start(bf16[336,128]{1,0:T(8,128)(2,1)S(1)} %get-tuple-element.27), channel_id=1, source_target_pairs={{0,24},{8,16},{16,8},{24,0},{1,25},{9,17},{17,9},{25,1},{2,26},{10... | collective-permute-start | bytes 258056 | tf_op jit(solution)/shard_map/ppermute | solution.py:606
  11.0 8.0 %collective-permute-start.1 = (bf16[336,128]{1,0:T(8,128)(2,1)S(1)}, bf16[336,128]{1,0:T(8,128)(2,1)S(1)}, u32[]{:S(2)}, u32[]{:S(2)}) collective-permute-start(bf16[336,128]{1,0:T(8,128)(2,1)S(1)} %get-tuple-element.28), channel_id=1, source_target_pairs={{0,16},{8,24},{16,0},{24,8},{1,17},{9,25},{17,1},{25,9},{2,18},{10... | collective-permute-start | bytes 258056 | tf_op jit(solution)/shard_map/ppermute | solution.py:606
  11.1 15.3 %copy-start = (bf16[576,288]{1,0:T(8,128)(2,1)S(1)}, bf16[576,288]{1,0:T(8,128)(2,1)}, u32[]{:S(2)}) copy-start(bf16[576,288]{1,0:T(8,128)(2,1)} %constant.123.refs_8_.usual_ref) | copy-start | bytes 995332
  11.1 15.3 %copy-start.3 = (bf16[576,288]{1,0:T(8,128)(2,1)S(1)}, bf16[576,288]{1,0:T(8,128)(2,1)}, u32[]{:S(2)}) copy-start(bf16[576,288]{1,0:T(8,128)(2,1)} %constant.124) | copy-start | bytes 995332
  19.3 4.9 %collective-permute-start.6 = (bf16[336,128]{1,0:T(8,128)(2,1)S(1)}, bf16[336,128]{1,0:T(8,128)(2,1)S(1)}, u32[]{:S(2)}, u32[]{:S(2)}) collective-permute-start(bf16[336,128]{1,0:T(8,128)(2,1)S(1)} %pad_maximum_fusion), channel_id=1, source_target_pairs={{0,4},{1,3},{2,6},{3,1},{4,0},{5,7},{6,2},{7,5},{8,12},{9,11},{10,... | collective-permute-start | bytes 258056 | tf_op jit(solution)/shard_map/ppermute | solution.py:626
  20.9 5.5 %collective-permute-start.8 = (bf16[336,128]{1,0:T(8,128)(2,1)S(1)}, bf16[336,128]{1,0:T(8,128)(2,1)S(1)}, u32[]{:S(2)}, u32[]{:S(2)}) collective-permute-start(bf16[336,128]{1,0:T(8,128)(2,1)S(1)} %pad_maximum_fusion.1), channel_id=1, source_target_pairs={{0,6},{1,7},{2,4},{3,5},{4,2},{5,3},{6,0},{7,1},{8,14},{9,15},{10,... | collective-permute-start | bytes 258056 | tf_op jit(solution)/shard_map/ppermute | solution.py:626
  22.4 4.4 %collective-permute-start.5 = (bf16[168,128]{1,0:T(8,128)(2,1)S(1)}, bf16[168,128]{1,0:T(8,128)(2,1)S(1)}, u32[]{:S(2)}, u32[]{:S(2)}) collective-permute-start(bf16[168,128]{1,0:T(8,128)(2,1)S(1)} %get-tuple-element.23), channel_id=1, source_target_pairs={{0,3},{1,4},{2,1},{3,6},{4,7},{5,0},{6,5},{7,2},{8,11},{9,12},{10,... | collective-permute-start | bytes 129032 | tf_op jit(solution)/shard_map/ppermute | solution.py:626
  22.7 4.1 %collective-permute-start.4 = (bf16[168,128]{1,0:T(8,128)(2,1)S(1)}, bf16[168,128]{1,0:T(8,128)(2,1)S(1)}, u32[]{:S(2)}, u32[]{:S(2)}) collective-permute-start(bf16[168,128]{1,0:T(8,128)(2,1)S(1)} %get-tuple-element.24), channel_id=1, source_target_pairs={{0,2},{1,5},{2,0},{3,7},{4,6},{5,1},{6,4},{7,3},{8,10},{9,13},{10,... | collective-permute-start | bytes 129032 | tf_op jit(solution)/shard_map/ppermute | solution.py:626
  23.2 3.5 %collective-permute-start.3 = (bf16[168,128]{1,0:T(8,128)(2,1)S(1)}, bf16[168,128]{1,0:T(8,128)(2,1)S(1)}, u32[]{:S(2)}, u32[]{:S(2)}) collective-permute-start(bf16[168,128]{1,0:T(8,128)(2,1)S(1)} %get-tuple-element.25), channel_id=1, source_target_pairs={{0,1},{1,0},{2,3},{3,2},{4,5},{5,4},{6,7},{7,6},{8,9},{9,8},{10,11... | collective-permute-start | bytes 129032 | tf_op jit(solution)/shard_map/ppermute | solution.py:626
  24.2 2.5 %collective-permute-start.7 = (bf16[168,128]{1,0:T(8,128)(2,1)S(1)}, bf16[168,128]{1,0:T(8,128)(2,1)S(1)}, u32[]{:S(2)}, u32[]{:S(2)}) collective-permute-start(bf16[168,128]{1,0:T(8,128)(2,1)S(1)} %slice.8), channel_id=1, source_target_pairs={{0,1},{1,0},{2,3},{3,2},{4,5},{5,4},{6,7},{7,6},{8,9},{9,8},{10,11... | collective-permute-start | bytes 129032 | tf_op jit(solution)/shard_map/ppermute | solution.py:626
  26.4 1.2 %collective-permute-start.9 = (bf16[168,128]{1,0:T(8,128)(2,1)S(1)}, bf16[168,128]{1,0:T(8,128)(2,1)S(1)}, u32[]{:S(2)}, u32[]{:S(2)}) collective-permute-start(bf16[168,128]{1,0:T(8,128)(2,1)S(1)} %slice.9), channel_id=1, source_target_pairs={{0,1},{1,0},{2,3},{3,2},{4,5},{5,4},{6,7},{7,6},{8,9},{9,8},{10,11... | collective-permute-start | bytes 129032 | tf_op jit(solution)/shard_map/ppermute | solution.py:626
  28.3 5.1 %copy-start.1 = (bf16[144,144]{1,0:T(8,128)(2,1)S(1)}, bf16[144,144]{1,0:T(8,128)(2,1)}, u32[]{:S(2)}) copy-start(bf16[144,144]{1,0:T(8,128)(2,1)} %constant.121.clone.order_ref.refs_4_) | copy-start | bytes 124420
  28.3 5.1 %copy-start.2 = (bf16[256,256]{1,0:T(8,128)(2,1)S(1)}, bf16[256,256]{1,0:T(8,128)(2,1)}, u32[]{:S(2)}) copy-start(bf16[256,256]{1,0:T(8,128)(2,1)} %constant.120.clone.unfold_ref) | copy-start | bytes 393220
  28.8 7.8 %collective-permute-start.12 = (bf16[328,128]{1,0:T(8,128)(2,1)S(1)}, bf16[328,128]{1,0:T(8,128)(2,1)S(1)}, u32[]{:S(2)}, u32[]{:S(2)}) collective-permute-start(bf16[328,128]{1,0:T(8,128)(2,1)S(1)} %get-tuple-element.31), channel_id=1, source_target_pairs={{0,24},{8,16},{16,8},{24,0},{1,25},{9,17},{17,9},{25,1},{2,26},{10... | collective-permute-start | bytes 251912 | tf_op jit(solution)/shard_map/ppermute | solution.py:606
  31.4 7.3 %collective-permute-start.10 = (bf16[328,128]{1,0:T(8,128)(2,1)S(1)}, bf16[328,128]{1,0:T(8,128)(2,1)S(1)}, u32[]{:S(2)}, u32[]{:S(2)}) collective-permute-start(bf16[328,128]{1,0:T(8,128)(2,1)S(1)} %get-tuple-element.33), channel_id=1, source_target_pairs={{0,8},{8,0},{16,24},{24,16},{1,9},{9,1},{17,25},{25,17},{2,10},{10... | collective-permute-start | bytes 251912 | tf_op jit(solution)/shard_map/ppermute | solution.py:606
  31.5 7.6 %collective-permute-start.11 = (bf16[328,128]{1,0:T(8,128)(2,1)S(1)}, bf16[328,128]{1,0:T(8,128)(2,1)S(1)}, u32[]{:S(2)}, u32[]{:S(2)}) collective-permute-start(bf16[328,128]{1,0:T(8,128)(2,1)S(1)} %get-tuple-element.32), channel_id=1, source_target_pairs={{0,16},{8,24},{16,0},{24,8},{1,17},{9,25},{17,1},{25,9},{2,18},{10... | collective-permute-start | bytes 251912 | tf_op jit(solution)/shard_map/ppermute | solution.py:606
